TPU v7x, 128 devices: a whole 4x4x4 slice. The times are simulated.
128 devices in a mesh: rep: 2 (over x_hi), fs: 16 (over y, x_lo, core), tp: 4 (over z).
Axes of the slice: x: 4 (x_hi: 2, x_lo: 2; x = x_hi * 2 + x_lo), y: 4, z: 4, core: 2. Of those that a mesh axis runs over, the one named last changes fastest.
Arguments:
- tokens: bfloat16 [16384, 2048], P(('rep', 'fs', 'tp')), may hold values from -3 to 3
- mixer_output: bfloat16 [16384, 2048], P(('rep', 'fs', 'tp')), may hold values from -6 to 6
- early_norm: float32 [2048], replicated, may hold values from 0.75 to 1.25
- early_gate: bfloat16 [2048, 5120], P('fs', 'tp'), may hold values from -0.125 to 0.125
- early_value: bfloat16 [2048, 5120], P('fs', 'tp'), may hold values from -0.125 to 0.125
- early_down: bfloat16 [5120, 2048], P('tp', 'fs'), may hold values from -0.078125 to 0.078125
- early_post: float32 [2048], replicated, may hold values from 0.75 to 1.25
- mixer_gain: float32 [2048], replicated, may hold values from 0.75 to 1.25
- later_norm: float32 [2048], replicated, may hold values from 0.75 to 1.25
- later_gate: bfloat16 [2048, 5120], P('fs', 'tp'), may hold values from -0.125 to 0.125
- later_value: bfloat16 [2048, 5120], P('fs', 'tp'), may hold values from -0.125 to 0.125
- later_down: bfloat16 [5120, 2048], P('tp', 'fs'), may hold values from -0.078125 to 0.078125
- later_post: float32 [2048], replicated, may hold values from 0.75 to 1.25
Outputs:
- layer_out: bfloat16 [16384, 2048], P(('rep', 'fs', 'tp'))
All inputs are finite; a program needn't handle non-finite values.
Results may differ from a plain program's by a relative error of at most 0.015.
Values may be sent and summed in bfloat16 or wider, within the bound.
A program may use at most 128 MiB of HBM per device.

v0:
```python
import functools

import jax
import jax.numpy as jnp
from jax import lax
from jax.experimental import pallas as pl
from jax.experimental.pallas import tpu as pltpu
from jax.sharding import PartitionSpec as P

epsilon = 1e-06
CORES = 2


def rms_scale(values, gain):
    scale = lax.rsqrt(jnp.mean(values * values, axis=-1, keepdims=True) + epsilon)
    return values * scale * gain


def kernel(
    R, F, T,
    tokens, mixer, early_norm, w0, w1, w2, early_post, mixer_gain, later_norm, w3, w4, w5, later_post,
    out,
    g0, g1, g2, g3, g4, g5, rows0, rows1, hidden, part, mixed, from_left, from_right,
    w_send, w_recv, local_sem, z_send, z_recv,
):
    source = (w0, w1, w2, w3, w4, w5)
    full = (g0, g1, g2, g3, g4, g5)
    all_rows = (rows0, rows1)
    r, f, t = lax.axis_index("rep"), lax.axis_index("fs"), lax.axis_index("tp")
    G = F // CORES
    g, c = f // CORES, f % CORES
    n, D = tokens.shape
    half = T // 2
    cut = D // 2
    mate = {"fs": g * CORES + 1 - c}
    ahead = {"fs": (g + 1) % G * CORES + c}
    behind = {"fs": (g + G - 1) % G * CORES + c}
    z_right, z_left = {"tp": (t + 1) % T}, {"tp": (t + T - 1) % T}
    peers = [{"rep": (r + k) % R} for k in range(1, R)]

    partners = [mate] + peers
    if G > 1:
        partners += [ahead] if G == 2 else [ahead, behind]
    partners += [z_right] if T == 2 else [z_right, z_left]
    barrier = pltpu.get_barrier_semaphore()
    for who in partners:
        pl.semaphore_signal(barrier, inc=1, device_id=who, device_id_type=pl.DeviceIdType.MESH)
    pl.semaphore_wait(barrier, len(partners))

    pending, done = [], set()

    def send(src, dst, sems, index, who):
        copy = pltpu.make_async_remote_copy(
            src_ref=src, dst_ref=dst, send_sem=sems[0].at[index], recv_sem=sems[1].at[index],
            device_id=who, device_id_type=pl.DeviceIdType.MESH,
        )
        copy.start()
        pending.append(copy)
        return copy

    slots = {}

    def w_index(*key):
        return slots.setdefault(key, len(slots))

    copies = {}

    def piece(m, shard, q):
        if m % 3 == 2:
            count = full[m].shape[1] // R
            return full[m].at[shard, pl.ds(pl.multiple_of(q * count, count), count)]
        depth = source[m].shape[0]
        count = depth // R
        return full[m].at[pl.ds(pl.multiple_of(shard * depth + q * count, count), count)]

    def whole_shard(m, shard):
        if m % 3 == 2:
            return full[m].at[shard]
        depth = source[m].shape[0]
        return full[m].at[pl.ds(pl.multiple_of(shard * depth, depth), depth)]

    W = (w_send, w_recv)

    def w_send_to(key, src, dst, who):
        copies[key] = send(src, dst, W, w_index(*key), who)

    def start_weights(m):
        if G > 1:
            count = source[m].shape[0] // R
            own = source[m].at[pl.ds(pl.multiple_of(r * count, count), count)]
            w_send_to(("ring", m, 1), own, piece(m, f, r), ahead)
        w_send_to(("own", m), source[m], whole_shard(m, f), mate)
        local = pltpu.make_async_copy(source[m], whole_shard(m, f), local_sem.at[m])
        local.start()
        copies["local", m] = local

    def ring_relay(m):
        for s in range(1, G):
            copies["ring", m, s].wait_recv()
            got = piece(m, (g + G - s) % G * CORES + c, r)
            if s < G - 1:
                w_send_to(("ring", m, s + 1), got, got, ahead)
            for k, who in enumerate(peers):
                w_send_to(("peer", m, s, k), got, got, who)
            w_send_to(("mate", m, s), got, got, mate)

    def peer_relay(m):
        for s in range(1, G):
            for k in range(len(peers)):
                copies["peer", m, s, k].wait_recv()
                got = piece(m, (g + G - s) % G * CORES + c, (r + R - 1 - k) % R)
                w_send_to(("pass", m, s, k), got, got, mate)

    def ready(m):
        copies["local", m].wait()
        copies["own", m].wait_recv()
        for s in range(1, G):
            copies["mate", m, s].wait_recv()
            for k in range(len(peers)):
                copies["pass", m, s, k].wait_recv()

    Z = (z_send, z_recv)

    def block(where, ref):
        return ref.at[pl.ds(pl.multiple_of(where * n, n), n)]

    def sides(ref, d):
        return (ref.at[:, :cut], ref.at[:, cut:]) if d == half else (ref, ref)

    def z_slot(phase, layer, step, way):
        return ((phase * 2 + layer) * half + step) * 2 + way

    def gather_send(layer, d):
        rows = all_rows[layer]
        a = sides(block((t + T - (d - 1)) % T, rows), d)[0]
        b = sides(block((t + d - 1) % T, rows), d)[1]
        copies["ag", layer, d] = (
            send(a, a, Z, z_slot(0, layer, d - 1, 0), z_right),
            send(b, b, Z, z_slot(0, layer, d - 1, 1), z_left),
        )

    def gather_wait(layer, d):
        for copy in copies["ag", layer, d]:
            copy.wait_recv()

    def sum_send(layer, k):
        d = half - k
        a = sides(block((t + d) % T, part), d)[0]
        b = sides(block((t + T - d) % T, part), d)[1]
        to_a = sides(from_left.at[layer * half + k], d)[0]
        to_b = sides(from_right.at[layer * half + k], d)[1]
        copies["rs", layer, k] = (
            send(a, to_a, Z, z_slot(1, layer, k, 0), z_right),
            send(b, to_b, Z, z_slot(1, layer, k, 1), z_left),
        )

    def sum_step(layer, k):
        for copy in copies["rs", layer, k - 1]:
            copy.wait_recv()
        d = half - k
        for way, where, buffer in ((0, (t + d) % T, from_left), (1, (t + T - d) % T, from_right)):
            mine = sides(block(where, part), d + 1)[way]
            came = sides(buffer.at[layer * half + k - 1], d + 1)[way]
            mine[...] = (mine[...].astype(jnp.float32) + came[...].astype(jnp.float32)).astype(jnp.bfloat16)
        sum_send(layer, k)

    def sum_own(layer):
        for copy in copies["rs", layer, half - 1]:
            copy.wait_recv()
        own = block(t, part)[...].astype(jnp.float32)
        a = from_left.at[layer * half + half - 1]
        b = from_right.at[layer * half + half - 1]
        if half > 1:
            return own + a[...].astype(jnp.float32) + b[...].astype(jnp.float32)
        came = jnp.concatenate([a[:, :cut], b[:, cut:]], axis=1)
        return own + came.astype(jnp.float32)

    def up(layer):
        gate, value = full[3 * layer], full[3 * layer + 1]
        wide = gate.shape[1]
        tile = 256 if wide % 256 == 0 else 128

        @pl.loop(0, wide // tile)
        def _(j):
            at = pl.ds(pl.multiple_of(j * tile, tile), tile)
            x = all_rows[layer][...]
            a = jnp.dot(x, gate[:, at], preferred_element_type=jnp.float32)
            b = jnp.dot(x, value[:, at], preferred_element_type=jnp.float32)
            hidden[:, at] = (a / (1.0 + jnp.exp(-a)) * b).astype(jnp.bfloat16)

    def down(layer):
        weight = full[3 * layer + 2]
        wide = weight.shape[2]
        tile = 256 if wide % 256 == 0 else 128
        per = wide // tile

        @pl.loop(0, F * per)
        def _(j):
            inside = pl.ds(pl.multiple_of(j % per * tile, tile), tile)
            at = pl.ds(pl.multiple_of(j * tile, tile), tile)
            y = jnp.dot(hidden[...], weight[j // per, :, inside], preferred_element_type=jnp.float32)
            part[:, at] = y.astype(jnp.bfloat16)

    start_weights(0)
    start_weights(1)
    block(t, rows0)[...] = rms_scale(tokens[...].astype(jnp.float32), early_norm[...]).astype(jnp.bfloat16)
    gather_send(0, 1)
    for m in range(2, 6):
        start_weights(m)
    ring_relay(0)
    for d in range(1, half):
        gather_wait(0, d)
        gather_send(0, d + 1)
    ring_relay(1)
    peer_relay(0)
    gather_wait(0, half)
    ring_relay(2)
    peer_relay(1)
    ready(0)
    ready(1)
    up(0)
    ring_relay(3)
    peer_relay(2)
    ready(2)
    down(0)
    sum_send(0, 0)
    for k in range(1, half):
        sum_step(0, k)
    ring_relay(4)
    peer_relay(3)
    branch = sum_own(0)
    keep = (
        tokens[...].astype(jnp.float32)
        + 0.5 * rms_scale(branch, early_post[...])
        + rms_scale(mixer[...].astype(jnp.float32), mixer_gain[...])
    ).astype(jnp.bfloat16)
    mixed[...] = keep
    block(t, rows1)[...] = rms_scale(keep.astype(jnp.float32), later_norm[...]).astype(jnp.bfloat16)
    gather_send(1, 1)
    for k in range(half):
        for copy in copies["rs", 0, k]:
            copy.wait_send()
            done.add(id(copy))
    ring_relay(5)
    peer_relay(4)
    for d in range(1, half):
        gather_wait(1, d)
        gather_send(1, d + 1)
    gather_wait(1, half)
    ready(3)
    ready(4)
    up(1)
    peer_relay(5)
    ready(5)
    down(1)
    sum_send(1, 0)
    for k in range(1, half):
        sum_step(1, k)
    branch = sum_own(1)
    out[...] = (
        mixed[...].astype(jnp.float32) + 0.5 * rms_scale(branch, later_post[...])
    ).astype(jnp.bfloat16)
    for copy in pending:
        if id(copy) not in done:
            copy.wait_send()


def on_device(sizes, *args):
    R, F, T = sizes
    (tokens, mixer, early_norm, eg, ev, ed, early_post, mixer_gain, later_norm, lg, lv, ld, later_post) = args
    n, D = tokens.shape
    depth, wide = eg.shape
    bf16 = jnp.bfloat16
    gains = [x.reshape(1, D) for x in (early_norm, early_post, mixer_gain, later_norm, later_post)]
    vmem = pl.BlockSpec(memory_space=pltpu.VMEM)
    hbm = pl.BlockSpec(memory_space=pl.ANY)
    gathered = [pltpu.VMEM((F * depth, wide), bf16)] * 2 + [pltpu.VMEM((F,) + ed.shape, bf16)]
    G = F // CORES
    w_count = 6 * (1 + (G - 1) * 2 * R)
    z_count = 4 * T
    return pl.pallas_call(
        functools.partial(kernel, R, F, T),
        out_shape=jax.ShapeDtypeStruct((n, D), bf16),
        in_specs=[vmem] * 3 + [hbm] * 3 + [vmem] * 3 + [hbm] * 3 + [vmem],
        out_specs=vmem,
        scratch_shapes=gathered * 2
        + [
            pltpu.VMEM((T * n, D), bf16),
            pltpu.VMEM((T * n, D), bf16),
            pltpu.VMEM((T * n, wide), bf16),
            pltpu.VMEM((T * n, D), bf16),
            pltpu.VMEM((n, D), bf16),
            pltpu.VMEM((T, n, D), bf16),
            pltpu.VMEM((T, n, D), bf16),
            pltpu.SemaphoreType.DMA((w_count,)),
            pltpu.SemaphoreType.DMA((w_count,)),
            pltpu.SemaphoreType.DMA((6,)),
            pltpu.SemaphoreType.DMA((z_count,)),
            pltpu.SemaphoreType.DMA((z_count,)),
        ],
        compiler_params=pltpu.CompilerParams(
            collective_id=0, has_side_effects=True, vmem_limit_bytes=66_000_000
        ),
    )(tokens, mixer, gains[0], eg, ev, ed, gains[1], gains[2], gains[3], lg, lv, ld, gains[4])


def solution(mesh):
    placed = (
        P(("rep", "fs", "tp"), None),
        P(("rep", "fs", "tp"), None),
        P(),
        P("fs", "tp"),
        P("fs", "tp"),
        P("tp", "fs"),
        P(),
        P(),
        P(),
        P("fs", "tp"),
        P("fs", "tp"),
        P("tp", "fs"),
        P(),
    )
    sizes = tuple(mesh.shape[name] for name in ("rep", "fs", "tp"))
    return jax.shard_map(
        functools.partial(on_device, sizes),
        mesh=mesh,
        in_specs=placed,
        out_specs=P(("rep", "fs", "tp"), None),
        check_vma=False,
    )
```

profile of v0, /device:TPU:0, one launch (start us, length us, event | category | flops | bytes accessed | tf_op | source)
XLA Modules:
  0.0 364.6 jit_solution(4681902702460007912)
XLA Ops:
  0.0 362.7 %shard_map.127 = bf16[128,2048]{1,0:T(8,128)(2,1)} custom-call(bf16[128,2048]{1,0:T(8,128)(2,1)} %tokens.1, bf16[128,2048]{1,0:T(8,128)(2,1)} %mixer.1, f32[1,2048]{1,0:T(1,128)} %bitcast.5, bf16[128,1280]{1,0:T(8,128)(2,1)} %w0.1, bf16[128,1280]{1,0:T(8,128)(2,1)} %w1.1, bf16[1280,128]{1,0:T(8,128)(2,1)} %w2.1, f32[1,2048]{1,0:T(1,128)} %bitcast.6, ...), custom_call_target="tpu_custom_call" | custom-call | tf_op jit(solution)/shard_map/pallas_call | solution.py:281
  362.7 1.9 copy.15
where the time goes:
time: 366 us; the launch traced here: 365 us
  Pallas kernels  363 us (99%)
    pallas_call x1, Pallas kernels, on_device(): pl.pallas_call(functools.partial(kernel, R, F, T), out_shape=jax.ShapeDty...  363 us

commit v1 on v0

v1 whole, which is shorter than its diff:
```python
import functools

import jax
import jax.numpy as jnp
from jax import lax
from jax.experimental import pallas as pl
from jax.experimental.pallas import tpu as pltpu
from jax.sharding import PartitionSpec as P

epsilon = 1e-06
GROUPS = ((0, 0), (1, 0), (3, 0), (0, 1), (2, 0), (3, 1), (1, 1), (2, 1))
TILE = 256
Y, X, T = 4, 4, 4

PIECES = {
    "ypA": (3, 0, 0, 2), "ypB": (3, 0, 2, 2), "ymA": (1, 0, 0, 2), "ymB": (1, 0, 2, 2),
    "fA": (2, 0, 0, 2), "fB": (2, 0, 2, 2),
    "xA": (0, 1, 0, 2), "xB": (0, 1, 2, 2),
    "qp": (3, 1, 0, 1), "qm": (1, 1, 2, 1),
    "x1a": (3, 1, 1, 1), "x1b": (3, 1, 2, 2), "x2a": (1, 1, 0, 2), "x2b": (1, 1, 3, 1),
    "x3a": (2, 1, 0, 2), "x3b": (2, 1, 2, 2),
}
ROUTES = {
    "ypA": ("y+", None), "ypB": ("y+", None), "ymA": ("y-", None), "ymB": ("y-", None),
    "xA": ("x+", None), "xB": ("x-", None),
    "fA": ("y+", "ypA"), "fB": ("y-", "ymB"),
    "qp": ("y+", "xA"), "qm": ("y-", "xB"),
    "x1a": ("x+", "ypA"), "x1b": ("x-", "ypB"), "x2a": ("x+", "ymA"), "x2b": ("x-", "ymB"),
    "x3a": ("x+", "fA"), "x3b": ("x-", "fB"),
}


def rms_scale(values, gain):
    scale = lax.rsqrt(jnp.mean(values * values, axis=-1, keepdims=True) + epsilon)
    return values * scale * gain


def kernel(
    tokens, mixer, early_norm, w0, w1, w2, early_post, mixer_gain, later_norm, w3, w4, w5, later_post,
    out,
    g0, g1, g2, g3, g4, g5, rows0, rows1, gate_sum, hidden, part, base, branch, mixed, from_far, from_short, from_long,
    w_send, w_recv, local_sem, z_send, z_recv,
):
    source = (w0, w1, w2, w3, w4, w5)
    full = (g0, g1, g2, g3, g4, g5)
    all_rows = (rows0, rows1)
    r, f, t = lax.axis_index("rep"), lax.axis_index("fs"), lax.axis_index("tp")
    c = f % 2
    xl = f // 2 % 2
    y = f // 4
    x = r * 2 + xl
    n, D = tokens.shape

    def chip(dx, dy):
        xx = (x + dx) % X
        return {"rep": xx // 2, "fs": ((y + dy) % Y * 2 + xx % 2) * 2 + c}

    where = {"y+": chip(0, 1), "y-": chip(0, Y - 1), "x+": chip(1, 0), "x-": chip(X - 1, 0)}
    mate = {"fs": f + 1 - 2 * c}
    z_right, z_left = {"tp": (t + 1) % T}, {"tp": (t + T - 1) % T}

    barrier = pltpu.get_barrier_semaphore()
    partners = [mate, *where.values(), z_right, z_left]
    for who in partners:
        pl.semaphore_signal(barrier, inc=1, device_id=who, device_id_type=pl.DeviceIdType.MESH)
    pl.semaphore_wait(barrier, len(partners))

    pending = []
    copies = {}
    counts = {"w": 0, "z": 0}

    def send(kind, key, src, dst, who):
        index = counts[kind]
        counts[kind] += 1
        sems = (w_send, w_recv) if kind == "w" else (z_send, z_recv)
        copy = pltpu.make_async_remote_copy(
            src_ref=src, dst_ref=dst, send_sem=sems[0].at[index], recv_sem=sems[1].at[index],
            device_id=who, device_id_type=pl.DeviceIdType.MESH,
        )
        copy.start()
        pending.append(copy)
        copies[key] = copy

    def owner(dy, other, core):
        return ((y + dy) % Y * 2 + (xl + other) % 2) * 2 + core

    def piece(m, shard, first, quarters):
        quarter = source[m].shape[0] // 4
        if m % 3 == 2:
            return full[m].at[shard, pl.ds(first * quarter, quarters * quarter)]
        start = pl.multiple_of(shard * 4 * quarter + first * quarter, quarter)
        return full[m].at[pl.ds(start, quarters * quarter)]

    def own_piece(m, name):
        quarter = source[m].shape[0] // 4
        _, _, first, quarters = PIECES[name]
        return source[m].at[pl.ds(first * quarter, quarters * quarter)]

    def pass_on(m, name):
        way, have = ROUTES[name]
        _, _, first, quarters = PIECES[name]
        if have is None:
            send("w", (name, m), own_piece(m, name), piece(m, f, first, quarters), where[way])
        else:
            dy, other, _, _ = PIECES[have]
            ref = piece(m, owner(dy, other, c), first, quarters)
            send("w", (name, m), ref, ref, where[way])

    def take(m, name, *onward):
        copies[name, m].wait_recv()
        for other in onward:
            pass_on(m, other)
        dy, column, first, quarters = PIECES[name]
        ref = piece(m, owner(dy, column, c), first, quarters)
        send("w", ("mate", name, m), ref, ref, mate)

    def own_y(m):
        for name in ("ypA", "ymB", "ypB", "ymA"):
            pass_on(m, name)

    def own_x(m):
        pass_on(m, "xA")
        pass_on(m, "xB")

    def own_mate(m):
        send("w", ("mate", "own", m), source[m], piece(m, f, 0, 4), mate)
        local = pltpu.make_async_copy(source[m], piece(m, f, 0, 4), local_sem.at[m])
        local.start()
        copies["local", m] = local

    def p1(m):
        take(m, "ypA", "fA", "x1a")
        take(m, "ymB", "fB", "x2b")

    def p2(m):
        take(m, "xA", "qp")
        take(m, "xB", "qm")

    def p3(m):
        take(m, "ypB", "x1b")
        take(m, "ymA", "x2a")

    def p4(m):
        take(m, "fA", "x3a")
        take(m, "fB", "x3b")

    def p5(m):
        for name in ("x1a", "x2b", "qp", "qm", "x1b", "x2a", "x3a", "x3b"):
            take(m, name)

    def ready(m, *groups):
        for dy, other in groups or GROUPS:
            if (dy, other) == (0, 0):
                copies["local", m].wait()
                copies["mate", "own", m].wait_recv()
            for name, (py, px, _, _) in PIECES.items():
                if (py, px) == (dy, other):
                    copies["mate", name, m].wait_recv()

    H = n // 2

    def row_half(ref, block, half):
        return ref.at[pl.ds(pl.multiple_of(block * n + half * H, H), H)]

    def gather_own(layer, half):
        ref = row_half(all_rows[layer], t, half)
        send("z", ("ag", layer, "r", half), ref, ref, z_right)
        send("z", ("ag", layer, "l", half), ref, ref, z_left)

    def gather_relay(layer):
        copies["ag", layer, "r", 0].wait_recv()
        ref = row_half(all_rows[layer], (t + T - 1) % T, 0)
        send("z", ("far", layer, 0), ref, ref, z_right)
        copies["ag", layer, "l", 1].wait_recv()
        ref = row_half(all_rows[layer], (t + 1) % T, 1)
        send("z", ("far", layer, 1), ref, ref, z_left)

    def gather_near(layer):
        copies["ag", layer, "r", 1].wait_recv()
        copies["ag", layer, "l", 0].wait_recv()

    def gather_far(layer):
        copies["far", layer, 0].wait_recv()
        copies["far", layer, 1].wait_recv()

    def gate(layer, first, last):
        weight = full[3 * layer]

        @pl.loop(first, last)
        def _(j):
            at = pl.ds(pl.multiple_of(j * TILE, TILE), TILE)
            gate_sum[:, at] = jnp.dot(all_rows[layer][...], weight[:, at], preferred_element_type=jnp.float32)

    def value(layer, first, last):
        weight = full[3 * layer + 1]

        @pl.loop(first, last)
        def _(j):
            at = pl.ds(pl.multiple_of(j * TILE, TILE), TILE)
            b = jnp.dot(all_rows[layer][...], weight[:, at], preferred_element_type=jnp.float32)
            a = gate_sum[:, at]
            hidden[:, at] = (a / (1.0 + jnp.exp(-a)) * b).astype(jnp.bfloat16)

    def block(layer, j, b):
        return part.at[layer, j, pl.ds(pl.multiple_of(b * n, n), n)]

    def down(layer, j):
        weight = full[3 * layer + 2]
        dy, other = GROUPS[j]
        both = jnp.concatenate([weight[owner(dy, other, 0)], weight[owner(dy, other, 1)]], axis=1)
        sums = jnp.dot(hidden[...], both, preferred_element_type=jnp.float32)
        part[layer, j] = sums.astype(jnp.bfloat16)
        long, short = (z_right, z_left) if j % 2 == 0 else (z_left, z_right)
        near = (t + T - 1) % T if j % 2 == 0 else (t + 1) % T
        send("z", ("rs2", layer, j), block(layer, j, (t + 2) % T), from_far.at[layer, j], long)
        send("z", ("rss", layer, j), block(layer, j, near), from_short.at[layer, j], short)

    def sum_step(layer, j):
        copies["rs2", layer, j].wait_recv()
        long, near = (z_right, (t + 1) % T) if j % 2 == 0 else (z_left, (t + T - 1) % T)
        mine = block(layer, j, near)
        mine[...] = (mine[...].astype(jnp.float32) + from_far[layer, j].astype(jnp.float32)).astype(jnp.bfloat16)
        send("z", ("rsl", layer, j), mine, from_long.at[layer, j], long)

    def sum_own(layer, j):
        copies["rss", layer, j].wait_recv()
        copies["rsl", layer, j].wait_recv()
        dy, other = GROUPS[j]
        at = pl.ds(pl.multiple_of(owner(dy, other, 0) * (D // 16), 2 * D // 16), 2 * D // 16)
        branch[:, at] = (
            block(layer, j, t)[...].astype(jnp.float32)
            + from_short[layer, j].astype(jnp.float32)
            + from_long[layer, j].astype(jnp.float32)
        )

    def finish_early(half):
        rows = pl.ds(half * H, H)
        keep = (base[rows] + 0.5 * rms_scale(branch[rows], early_post[...])).astype(jnp.bfloat16)
        mixed[rows] = keep
        row_half(rows1, t, half)[...] = rms_scale(keep.astype(jnp.float32), later_norm[...]).astype(jnp.bfloat16)
        gather_own(1, half)

    tiles = hidden.shape[1] // TILE

    own_y(0)
    own_x(0)
    own_x(1)
    own_mate(0)
    own_mate(1)
    for half in range(2):
        rows = pl.ds(half * H, H)
        row_half(rows0, t, half)[...] = rms_scale(tokens[rows].astype(jnp.float32), early_norm[...]).astype(jnp.bfloat16)
        gather_own(0, half)
    p1(0)
    p2(0)
    own_y(1)
    gather_relay(0)
    p3(0)
    own_x(2)
    own_mate(2)
    p4(0)
    base[...] = tokens[...].astype(jnp.float32) + rms_scale(mixer[...].astype(jnp.float32), mixer_gain[...])
    gather_near(0)
    p1(1)
    p2(1)
    own_y(2)
    p5(0)
    gather_far(0)
    ready(0)
    gate(0, 0, 2)
    p3(1)
    own_x(3)
    own_mate(3)
    gate(0, 2, tiles)
    p4(1)
    p1(2)
    p2(2)
    own_y(3)
    p5(1)
    ready(1)
    value(0, 0, 2)
    p3(2)
    own_x(4)
    own_mate(4)
    value(0, 2, tiles)
    ready(2, *GROUPS[:4])
    down(0, 0)
    down(0, 1)
    p4(2)
    down(0, 2)
    down(0, 3)
    sum_step(0, 0)
    sum_step(0, 1)
    ready(2, GROUPS[4])
    down(0, 4)
    p1(3)
    p2(3)
    own_y(4)
    sum_step(0, 2)
    sum_step(0, 3)
    p5(2)
    ready(2, *GROUPS[5:])
    down(0, 5)
    p3(3)
    own_x(5)
    own_mate(5)
    down(0, 6)
    down(0, 7)
    sum_step(0, 4)
    for j in range(4):
        sum_own(0, j)
    p4(3)
    for j in range(5, 8):
        sum_step(0, j)
    for j in range(4, 8):
        sum_own(0, j)
    finish_early(0)
    finish_early(1)
    p1(4)
    p2(4)
    own_y(5)
    p5(3)
    p3(4)
    p4(4)
    gather_relay(1)
    ready(3)
    gather_near(1)
    p1(5)
    p2(5)
    p5(4)
    ready(4)
    p3(5)
    gather_far(1)
    gate(1, 0, tiles)
    p4(5)
    value(1, 0, tiles)
    ready(5, *GROUPS[:5])
    for j in range(4):
        down(1, j)
    p5(5)
    sum_step(1, 0)
    sum_step(1, 1)
    down(1, 4)
    ready(5, *GROUPS[5:])
    down(1, 5)
    sum_step(1, 2)
    sum_step(1, 3)
    down(1, 6)
    down(1, 7)
    for j in range(4):
        sum_step(1, 4 + j)
        sum_own(1, j)
    for j in range(4, 8):
        sum_own(1, j)
    out[...] = (
        mixed[...].astype(jnp.float32) + 0.5 * rms_scale(branch[...], later_post[...])
    ).astype(jnp.bfloat16)
    for copy in pending:
        copy.wait_send()


def on_device(*args):
    (tokens, mixer, early_norm, eg, ev, ed, early_post, mixer_gain, later_norm, lg, lv, ld, later_post) = args
    n, D = tokens.shape
    depth, wide = eg.shape
    F = D // depth
    bf16, f32 = jnp.bfloat16, jnp.float32
    gains = [x.reshape(1, D) for x in (early_norm, early_post, mixer_gain, later_norm, later_post)]
    vmem = pl.BlockSpec(memory_space=pltpu.VMEM)
    hbm = pl.BlockSpec(memory_space=pl.ANY)
    gathered = [pltpu.VMEM((F * depth, wide), bf16)] * 2 + [pltpu.VMEM((F,) + ed.shape, bf16)]
    w_count = 6 * (2 * len(PIECES) + 1)
    z_count = 2 * (6 + 3 * len(GROUPS))
    landing = pltpu.VMEM((2, len(GROUPS), n, TILE), bf16)
    return pl.pallas_call(
        kernel,
        out_shape=jax.ShapeDtypeStruct((n, D), bf16),
        in_specs=[vmem] * 3 + [hbm] * 3 + [vmem] * 3 + [hbm] * 3 + [vmem],
        out_specs=vmem,
        scratch_shapes=gathered * 2
        + [
            pltpu.VMEM((T * n, D), bf16),
            pltpu.VMEM((T * n, D), bf16),
            pltpu.VMEM((T * n, wide), f32),
            pltpu.VMEM((T * n, wide), bf16),
            pltpu.VMEM((2, len(GROUPS), T * n, TILE), bf16),
            pltpu.VMEM((n, D), f32),
            pltpu.VMEM((n, D), f32),
            pltpu.VMEM((n, D), bf16),
            landing,
            landing,
            landing,
            pltpu.SemaphoreType.DMA((w_count,)),
            pltpu.SemaphoreType.DMA((w_count,)),
            pltpu.SemaphoreType.DMA((6,)),
            pltpu.SemaphoreType.DMA((z_count,)),
            pltpu.SemaphoreType.DMA((z_count,)),
        ],
        compiler_params=pltpu.CompilerParams(
            collective_id=0, has_side_effects=True, vmem_limit_bytes=66_000_000
        ),
    )(tokens, mixer, gains[0], eg, ev, ed, gains[1], gains[2], gains[3], lg, lv, ld, gains[4])


def solution(mesh):
    assert dict(mesh.shape) == {"rep": 2, "fs": 16, "tp": 4}
    rows = P(("rep", "fs", "tp"), None)
    up, down = P("fs", "tp"), P("tp", "fs")
    placed = (rows, rows, P(), up, up, down, P(), P(), P(), up, up, down, P())
    return jax.shard_map(on_device, mesh=mesh, in_specs=placed, out_specs=rows, check_vma=False)
```

time: 366 us -> 134 us (0.37)
  Pallas kernels: 363 us -> 132 us
    pallas_call x1, Pallas kernels: 363 us -> 132 us  [on_device(): pl.pallas_call(kernel, out_shape=jax.ShapeDtypeStruct((n, D), bf16), in_s...]
where the time goes in v1:
time: 134 us
  Pallas kernels  132 us (99%)
  local copies, waits for them, and re-layouts  1.88 us (1%)
    pallas_call x1, Pallas kernels, on_device(): pl.pallas_call(kernel, out_shape=jax.ShapeDtypeStruct((n, D), bf16), in_s...  132 us

profile of v1, /device:TPU:0, one launch (start us, length us, event | category | flops | bytes accessed | tf_op | source)
XLA Modules:
  0.0 134.2 jit_solution(15098961208068499809)
XLA Ops:
  0.0 132.3 %shard_map.127 = bf16[128,2048]{1,0:T(8,128)(2,1)} custom-call(bf16[128,2048]{1,0:T(8,128)(2,1)} %tokens.1, bf16[128,2048]{1,0:T(8,128)(2,1)} %mixer.1, f32[1,2048]{1,0:T(1,128)} %bitcast.5, bf16[128,1280]{1,0:T(8,128)(2,1)} %w0.1, bf16[128,1280]{1,0:T(8,128)(2,1)} %w1.1, bf16[1280,128]{1,0:T(8,128)(2,1)} %w2.1, f32[1,2048]{1,0:T(1,128)} %bitcast.6, ...), custom_call_target="tpu_custom_call" | custom-call | tf_op jit(solution)/shard_map/pallas_call | solution.py:375
  132.3 1.9 %copy.15 = bf16[128,2048]{1,0:T(8,128)(2,1)} copy(bf16[128,2048]{1,0:T(8,128)(2,1)} %shard_map.127) | data formatting | bytes 1048576

commit v2 on v1

v2 whole, which is shorter than its diff:
```python
import functools

import jax
import jax.numpy as jnp
from jax import lax
from jax.experimental import pallas as pl
from jax.experimental.pallas import tpu as pltpu
from jax.sharding import PartitionSpec as P

epsilon = 1e-06
TILE = 256
Y, X, T = 4, 4, 4
MATRICES = 6

(
    OY1, OY2, OY3, OX1, OX2, F1, F2, X1, X3, QQ, E1, E2, OM, A2, A3, B2, C2, D1, D2, D3, D4, G1Z, G1ZM, G2Z,
    G2ZM, G3Z, G3ZM, S2, SS, ADD, OWN, FIN, GATE0, VALUE0, DOWN0, GATE1, VALUE1, DOWN1,
) = range(38)

ORDER = (
    (G1Z, 0, 0), (G1ZM, 0, 0), (OY1, 0), (OM, 0), (OY2, 0), (OX1, 0), (OX2, 0), (G2Z, 0, 0), (G2ZM, 0, 0),
    (OY3, 0), (OX1, 1), (OX2, 1), (G1Z, 0, 1), (G1ZM, 0, 1), (OY1, 1), (OM, 1), (OX1, 2), (A2, 0), (B2, 0),
    (G3Z, 0, 0), (G3ZM, 0, 0), (OY2, 1), (X1, 0), (F1, 0), (OX2, 2), (A3, 0), (B2, 1), (G2Z, 0, 1),
    (G2ZM, 0, 1), (F2, 0), (X3, 0), (G3Z, 0, 1), (G3ZM, 0, 1), (OY3, 1), (A2, 1), (D1, 0), (X1, 1), (B2, 2),
    (F1, 1), (E1, 0), (C2, 0), (F2, 1), (E2, 0), (D3, 0), (QQ, 0), (OX1, 3), (A3, 1), (D1, 1), (QQ, 1), (X3, 1),
    (OY1, 2), (OM, 2), (C2, 1), (D4, 0), (OY2, 2), (E1, 1), (D2, 0), (OY3, 2), (GATE0, 0, 1), (D2, 1), (E2, 1),
    (GATE0, 1, 3), (OX2, 3), (GATE0, 3, 4), (D3, 1), (GATE0, 4, 5), (F1, 2), (OX1, 4), (A2, 2), (F2, 2),
    (X1, 2), (D4, 1), (QQ, 2), (OX2, 4), (A3, 2), (VALUE0, 0, 1), (B2, 3), (VALUE0, 1, 2), (X3, 2), (OY1, 3),
    (OM, 3), (VALUE0, 2, 4), (OY2, 3), (VALUE0, 4, 5), (C2, 2), (D1, 2), (DOWN0, 0), (S2, 0, 0, 0),
    (SS, 0, 0, 0), (S2, 0, 0, 1), (SS, 0, 0, 1), (E1, 2), (OY3, 3), (DOWN0, 1), (D2, 2), (B2, 4), (S2, 0, 1, 0),
    (SS, 0, 1, 0), (E2, 2), (SS, 0, 1, 1), (S2, 0, 1, 1), (ADD, 0, 0, 0), (F1, 3), (OX1, 5), (A2, 3), (D3, 2),
    (ADD, 0, 0, 1), (F2, 3), (X1, 3), (ADD, 0, 1, 0), (DOWN0, 2), (S2, 0, 2, 0), (SS, 0, 2, 0), (SS, 0, 2, 1),
    (QQ, 3), (OX2, 5), (A3, 3), (ADD, 0, 1, 1), (D4, 2), (S2, 0, 2, 1), (OY1, 4), (OM, 4), (OWN, 0, 0, 0),
    (X3, 3), (OWN, 0, 1, 0), (DOWN0, 3), (S2, 0, 3, 0), (SS, 0, 3, 0), (SS, 0, 3, 1), (OY2, 4), (OWN, 0, 0, 1),
    (C2, 3), (D1, 3), (S2, 0, 3, 1), (ADD, 0, 2, 0), (OY3, 4), (E1, 3), (D2, 3), (B2, 5), (ADD, 0, 2, 1),
    (OWN, 0, 1, 1), (E2, 3), (ADD, 0, 3, 0), (F1, 4), (A2, 4), (X1, 4), (D3, 3), (ADD, 0, 3, 1), (OWN, 0, 2, 0),
    (F2, 4), (OWN, 0, 3, 0), (FIN, 0, 0), (G1Z, 1, 0), (G1ZM, 1, 0), (QQ, 4), (OWN, 0, 2, 1), (A3, 4), (X3, 4),
    (D4, 3), (OWN, 0, 3, 1), (FIN, 0, 1), (G2Z, 1, 0), (G2ZM, 1, 0), (OY1, 5), (OM, 5), (E1, 4), (D1, 4),
    (OY2, 5), (G1Z, 1, 1), (G1ZM, 1, 1), (C2, 4), (E2, 4), (OY3, 5), (D2, 4), (D3, 4), (G3Z, 1, 0),
    (G3ZM, 1, 0), (F1, 5), (A2, 5), (X1, 5), (G2Z, 1, 1), (G2ZM, 1, 1), (D4, 4), (F2, 5), (G3Z, 1, 1),
    (G3ZM, 1, 1), (QQ, 5), (A3, 5), (X3, 5), (D1, 5), (GATE1, 0, 0, 4), (E1, 5), (GATE1, 0, 4, 5),
    (VALUE1, 0, 0, 3), (C2, 5), (E2, 5), (VALUE1, 0, 3, 5), (DOWN1, 0, 0), (S2, 1, 0, 0), (SS, 1, 0, 0),
    (DOWN1, 1, 0), (D2, 5), (D3, 5), (S2, 1, 1, 0), (SS, 1, 1, 0), (GATE1, 1, 0, 4), (DOWN1, 2, 0),
    (S2, 1, 2, 0), (SS, 1, 2, 0), (GATE1, 1, 4, 5), (ADD, 1, 0, 0), (VALUE1, 1, 0, 1), (D4, 5),
    (VALUE1, 1, 1, 3), (ADD, 1, 1, 0), (VALUE1, 1, 3, 5), (DOWN1, 3, 0), (ADD, 1, 2, 0), (S2, 1, 3, 0),
    (SS, 1, 3, 0), (DOWN1, 0, 1), (SS, 1, 0, 1), (DOWN1, 1, 1), (S2, 1, 0, 1), (S2, 1, 1, 1), (DOWN1, 2, 1),
    (OWN, 1, 0, 0), (DOWN1, 3, 1), (S2, 1, 2, 1), (S2, 1, 3, 1), (OWN, 1, 1, 0), (OWN, 1, 2, 0), (ADD, 1, 3, 0),
    (SS, 1, 1, 1), (SS, 1, 3, 1), (SS, 1, 2, 1), (ADD, 1, 0, 1), (ADD, 1, 1, 1), (ADD, 1, 2, 1), (ADD, 1, 3, 1),
    (OWN, 1, 3, 0), (FIN, 1, 0), (OWN, 1, 0, 1), (OWN, 1, 1, 1), (OWN, 1, 2, 1), (OWN, 1, 3, 1), (FIN, 1, 1),
)

SETS = (((0, 0), (3, 0)), ((1, 0), (0, 1)), ((2, 0), (3, 1)), ((1, 1), (2, 1)))
SET_OF = {chip: s for s, chips in enumerate(SETS) for chip in chips}
STEPS = {
    OY1: ((), (("y+", (0, 0), 0, 1), ("y-", (0, 0), 2, 1)), "W1"),
    OY2: ((), (("y+", (0, 0), 1, 1), ("y-", (0, 0), 3, 1)), "W2"),
    OY3: ((), (("y+", (0, 0), 2, 2), ("y-", (0, 0), 0, 2)), "W3"),
    OX1: ((), (("x+", (0, 0), 0, 1), ("x-", (0, 0), 2, 1)), "X1"),
    OX2: ((), (("x+", (0, 0), 1, 1), ("x-", (0, 0), 3, 1)), "X2"),
    F1: (("W1",), (("y+", (3, 0), 0, 1), ("y-", (1, 0), 2, 1)), "F1"),
    F2: (("W2",), (("y+", (3, 0), 1, 1), ("y-", (1, 0), 3, 1)), "F2"),
    X1: (("W2",), (("x+", (3, 0), 1, 1), ("x-", (1, 0), 3, 1)), "D1"),
    X3: (("W3",), (("x-", (3, 0), 2, 2), ("x+", (1, 0), 0, 2)), "D3"),
    QQ: (("X1",), (("y+", (0, 1), 0, 1), ("y-", (0, 1), 2, 1)), "D2"),
    E1: (("F1",), (("x+", (2, 0), 0, 1), ("x-", (2, 0), 2, 1)), "E1"),
    E2: (("F2",), (("x+", (2, 0), 1, 1), ("x-", (2, 0), 3, 1)), "E2"),
    OM: ((), (("mate", (0, 0), 0, 4),), None),
    A2: (("W1", "W2"), (("mate", (3, 0), 0, 2), ("mate", (1, 0), 2, 2)), None),
    A3: (("W3",), (("mate", (3, 0), 2, 2), ("mate", (1, 0), 0, 2)), None),
    B2: (("X1", "X2"), (("mate", (0, 1), 0, 4),), None),
    C2: (("F1", "F2"), (("mate", (2, 0), 0, 4),), None),
    D1: (("D1",), (("mate", (3, 1), 1, 1), ("mate", (1, 1), 3, 1)), None),
    D2: (("D2",), (("mate", (3, 1), 0, 1), ("mate", (1, 1), 2, 1)), None),
    D3: (("D3",), (("mate", (3, 1), 2, 2), ("mate", (1, 1), 0, 2)), None),
    D4: (("E1", "E2"), (("mate", (2, 1), 0, 4),), None),
}
ARRIVALS = {arrival: sum(c[3] for c in moves) for _, moves, arrival in STEPS.values() if arrival}
SENT = sum(c[3] for _, moves, _ in STEPS.values() for c in moves)


def rms_scale(values, gain):
    scale = lax.rsqrt(jnp.mean(values * values, axis=-1, keepdims=True) + epsilon)
    return values * scale * gain


def kernel(
    tokens, mixer, early_norm, w0, w1, w2, early_post, mixer_gain, later_norm, w3, w4, w5, later_post,
    out,
    g0, g1, g2, g3, g4, g5, rows0, rows1, gate_sum, hidden, part, base, branch, mixed, from_far, from_short, from_long,
    w_send, w_recv, local_sem, z_send, z_recv,
):
    source = (w0, w1, w2, w3, w4, w5)
    full = (g0, g1, g2, g3, g4, g5)
    all_rows = (rows0, rows1)
    r, f, t = lax.axis_index("rep"), lax.axis_index("fs"), lax.axis_index("tp")
    c = f % 2
    xl = f // 2 % 2
    y = f // 4
    x = r * 2 + xl
    n, D = tokens.shape
    H = n // 2
    M = T * H
    U = H // 2

    def chip(dx, dy):
        xx = (x + dx) % X
        return {"rep": xx // 2, "fs": ((y + dy) % Y * 2 + xx % 2) * 2 + c}

    where = {
        "y+": chip(0, 1), "y-": chip(0, Y - 1), "x+": chip(1, 0), "x-": chip(X - 1, 0),
        "mate": {"fs": f + 1 - 2 * c}, "z+": {"tp": (t + 1) % T}, "z-": {"tp": (t + T - 1) % T},
    }

    def owner(chip, core):
        dy, other = chip
        return ((y + dy) % Y * 2 + (xl + other) % 2) * 2 + core

    def piece(m, shard, first, quarters):
        quarter = source[m].shape[0] // 4
        if m % 3 == 2:
            return full[m].at[shard, pl.ds(first * quarter, quarters * quarter)]
        start = pl.multiple_of(shard * 4 * quarter + first * quarter, quarter)
        return full[m].at[pl.ds(start, quarters * quarter)]

    def some(m, quarters):
        if m % 3 == 2:
            if quarters % 4 == 0:
                return full[m].at[pl.ds(0, quarters // 4)]
            return full[m].at[0, pl.ds(0, quarters * (source[m].shape[0] // 4))]
        return full[m].at[pl.ds(0, quarters * (source[m].shape[0] // 4))]

    barrier = pltpu.get_barrier_semaphore()
    for who in where.values():
        pl.semaphore_signal(barrier, inc=1, device_id=who, device_id_type=pl.DeviceIdType.MESH)
    local = []
    for m in range(MATRICES):
        local.append(pltpu.make_async_copy(source[m], piece(m, f, 0, 4), local_sem.at[m]))
        local[m].start()

    def own_rows(layer, half):
        return all_rows[layer].at[pl.ds(pl.multiple_of(half * M + t * H, H), H)]

    for half in range(2):
        at = pl.ds(half * H, H)
        own_rows(0, half)[...] = rms_scale(tokens[at].astype(jnp.float32), early_norm[...]).astype(jnp.bfloat16)
    base[...] = tokens[...].astype(jnp.float32) + rms_scale(mixer[...].astype(jnp.float32), mixer_gain[...])
    for m in range(MATRICES):
        local[m].wait()
    pl.semaphore_wait(barrier, len(where))

    slots = {"w": {}, "z": {}}
    arrived = set()

    def slot(kind, key):
        return slots[kind].setdefault(key, len(slots[kind]))

    def send(kind, src, dst, out_slot, key, way):
        sems = (w_send, w_recv) if kind == "w" else (z_send, z_recv)
        pltpu.make_async_remote_copy(
            src_ref=src, dst_ref=dst, send_sem=sems[0].at[out_slot], recv_sem=sems[1].at[slot(kind, key)],
            device_id=where[way], device_id_type=pl.DeviceIdType.MESH,
        ).start()

    def need(kind, key, same_bytes):
        if key not in arrived:
            arrived.add(key)
            sem = (w_recv if kind == "w" else z_recv).at[slot(kind, key)]
            pltpu.make_async_copy(same_bytes, same_bytes, sem).wait()

    def weights(name, m):
        waits, moves, arrival = STEPS[name]
        for key in waits:
            need("w", (key, m), some(m, ARRIVALS[key]))
        for way, chip, first, quarters in moves:
            ref = piece(m, owner(chip, c), first, quarters)
            key = arrival or ("mate", SET_OF[chip] if m % 3 == 2 else None)
            send("w", ref, ref, m, (key, m), way)

    def ready(m, s=None):
        if s is None:
            need("w", (("mate", None), m), some(m, 32))
        else:
            need("w", (("mate", s), m), some(m, 8))

    def row_piece(layer, half, block, u):
        start = pl.multiple_of(half * M + block % T * H + u * U, U)
        return all_rows[layer].at[pl.ds(start, U)]

    def gather(step, way, layer, half):
        u = (0 if way == "z+" else 1) if step != 2 else (1 if way == "z+" else 0)
        block = t
        if step == 3:
            gathered(1, layer, half)
            block = t + T - 1 if way == "z+" else t + 1
        ref = row_piece(layer, half, block, u)
        send("z", ref, ref, layer, ("rows", step, layer, half), way)

    def gathered(step, layer, half):
        need("z", ("rows", step, layer, half), all_rows[layer].at[pl.ds(0, 2 * U)])

    def all_gathered(layer, half):
        for step in (1, 2, 3):
            gathered(step, layer, half)

    def span(rows):
        return pl.ds(0, 2 * M) if rows is None else pl.ds(rows * M, M)

    def gate(layer, rows, first, last):
        weight = full[3 * layer]
        ready(3 * layer)
        for half in range(2) if rows is None else (rows,):
            all_gathered(layer, half)

        @pl.loop(first, last)
        def _(j):
            at = pl.ds(pl.multiple_of(j * TILE, TILE), TILE)
            gate_sum[span(rows), at] = jnp.dot(
                all_rows[layer][span(rows)], weight[:, at], preferred_element_type=jnp.float32
            )

    def value(layer, rows, first, last):
        weight = full[3 * layer + 1]
        ready(3 * layer + 1)

        @pl.loop(first, last)
        def _(j):
            at = pl.ds(pl.multiple_of(j * TILE, TILE), TILE)
            b = jnp.dot(all_rows[layer][span(rows)], weight[:, at], preferred_element_type=jnp.float32)
            a = gate_sum[span(rows), at]
            hidden[span(rows), at] = (a / (1.0 + jnp.exp(-a)) * b).astype(jnp.bfloat16)

    def down(layer, s, rows):
        weight = full[3 * layer + 2]
        ready(3 * layer + 2, s)
        for k, chip in enumerate(SETS[s]):
            both = jnp.concatenate([weight[owner(chip, 0)], weight[owner(chip, 1)]], axis=1)
            sums = jnp.dot(hidden[span(rows)], both, preferred_element_type=jnp.float32)
            part[layer, s, span(rows), pl.ds(k * TILE, TILE)] = sums.astype(jnp.bfloat16)

    def block(layer, s, half, b):
        return part.at[layer, s, pl.ds(pl.multiple_of(half * M + b % T * H, H), H)]

    def ways(s):
        right, left = ("z+", t + 1), ("z-", t + T - 1)
        return right + left if s % 2 == 0 else left + right

    def sum_far(layer, s, half):
        key = ("far", layer, s, half)
        send("z", block(layer, s, half, t + 2), from_far.at[layer, s, half], 2 + layer, key, ways(s)[0])

    def sum_short(layer, s, half):
        _, _, way, near = ways(s)
        key = ("own", layer, s, half)
        send("z", block(layer, s, half, near), from_short.at[layer, s, half], 2 + layer, key, way)

    def sum_long(layer, s, half):
        need("z", ("far", layer, s, half), from_far.at[layer, s, half])
        way, near, _, _ = ways(s)
        mine = block(layer, s, half, near)
        came = from_far[layer, s, half].astype(jnp.float32)
        mine[...] = (mine[...].astype(jnp.float32) + came).astype(jnp.bfloat16)
        send("z", mine, from_long.at[layer, s, half], 2 + layer, ("own", layer, s, half), way)

    def sum_own(layer, s, half):
        need("z", ("own", layer, s, half), part.at[layer, s, pl.ds(0, 2 * H)])
        total = (
            block(layer, s, half, t)[...].astype(jnp.float32)
            + from_short[layer, s, half].astype(jnp.float32)
            + from_long[layer, s, half].astype(jnp.float32)
        )
        for k, chip in enumerate(SETS[s]):
            at = pl.ds(pl.multiple_of(owner(chip, 0) * (TILE // 2), TILE), TILE)
            branch[pl.ds(half * H, H), at] = total[:, k * TILE : (k + 1) * TILE]

    def finish(layer, half):
        at = pl.ds(half * H, H)
        if layer == 0:
            keep = (base[at] + 0.5 * rms_scale(branch[at], early_post[...])).astype(jnp.bfloat16)
            mixed[at] = keep
            own_rows(1, half)[...] = rms_scale(keep.astype(jnp.float32), later_norm[...]).astype(jnp.bfloat16)
        else:
            out[at] = (
                mixed[at].astype(jnp.float32) + 0.5 * rms_scale(branch[at], later_post[...])
            ).astype(jnp.bfloat16)

    actions = {
        GATE0: lambda a, b: gate(0, None, a, b), VALUE0: lambda a, b: value(0, None, a, b),
        GATE1: lambda h, a, b: gate(1, h, a, b), VALUE1: lambda h, a, b: value(1, h, a, b),
        DOWN0: lambda s: down(0, s, None), DOWN1: lambda s, h: down(1, s, h),
        S2: sum_far, SS: sum_short, ADD: sum_long, OWN: sum_own, FIN: finish,
        G1Z: functools.partial(gather, 1, "z+"), G1ZM: functools.partial(gather, 1, "z-"),
        G2Z: functools.partial(gather, 2, "z+"), G2ZM: functools.partial(gather, 2, "z-"),
        G3Z: functools.partial(gather, 3, "z+"), G3ZM: functools.partial(gather, 3, "z-"),
    }
    for kind in STEPS:
        actions[kind] = functools.partial(weights, kind)
    for kind, *numbers in ORDER:
        actions[kind](*numbers)

    for m in range(MATRICES):
        pltpu.make_async_copy(some(m, SENT), some(m, SENT), w_send.at[m]).wait()
    for layer in range(2):
        sent = all_rows[layer].at[pl.ds(0, 12 * U)]
        pltpu.make_async_copy(sent, sent, z_send.at[layer]).wait()
        sent = part.at[layer, pl.ds(0, 3)]
        pltpu.make_async_copy(sent, sent, z_send.at[2 + layer]).wait()


def on_device(*args):
    (tokens, mixer, early_norm, eg, ev, ed, early_post, mixer_gain, later_norm, lg, lv, ld, later_post) = args
    n, D = tokens.shape
    depth, wide = eg.shape
    F = D // depth
    H = n // 2
    bf16, f32 = jnp.bfloat16, jnp.float32
    gains = [x.reshape(1, D) for x in (early_norm, early_post, mixer_gain, later_norm, later_post)]
    vmem = pl.BlockSpec(memory_space=pltpu.VMEM)
    hbm = pl.BlockSpec(memory_space=pl.ANY)
    gathered = [pltpu.VMEM((F * depth, wide), bf16)] * 2 + [pltpu.VMEM((F,) + ed.shape, bf16)]
    landing = pltpu.VMEM((2, len(SETS), 2, H, 2 * TILE), bf16)
    w_count = MATRICES * len(ARRIVALS) + 4 + 2 * len(SETS)
    z_count = 2 * 2 * (3 + 2 * len(SETS))
    return pl.pallas_call(
        kernel,
        out_shape=jax.ShapeDtypeStruct((n, D), bf16),
        in_specs=[vmem] * 3 + [hbm] * 3 + [vmem] * 3 + [hbm] * 3 + [vmem],
        out_specs=vmem,
        scratch_shapes=gathered * 2
        + [
            pltpu.VMEM((T * n, D), bf16),
            pltpu.VMEM((T * n, D), bf16),
            pltpu.VMEM((T * n, wide), f32),
            pltpu.VMEM((T * n, wide), bf16),
            pltpu.VMEM((2, len(SETS), T * n, 2 * TILE), bf16),
            pltpu.VMEM((n, D), f32),
            pltpu.VMEM((n, D), f32),
            pltpu.VMEM((n, D), bf16),
            landing,
            landing,
            landing,
            pltpu.SemaphoreType.DMA((MATRICES,)),
            pltpu.SemaphoreType.DMA((w_count,)),
            pltpu.SemaphoreType.DMA((MATRICES,)),
            pltpu.SemaphoreType.DMA((4,)),
            pltpu.SemaphoreType.DMA((z_count,)),
        ],
        compiler_params=pltpu.CompilerParams(
            collective_id=0, has_side_effects=True, vmem_limit_bytes=66_000_000
        ),
    )(tokens, mixer, gains[0], eg, ev, ed, gains[1], gains[2], gains[3], lg, lv, ld, gains[4])


def solution(mesh):
    assert dict(mesh.shape) == {"rep": 2, "fs": 16, "tp": 4}
    rows = P(("rep", "fs", "tp"), None)
    up, down = P("fs", "tp"), P("tp", "fs")
    placed = (rows, rows, P(), up, up, down, P(), P(), P(), up, up, down, P())
    return jax.shard_map(on_device, mesh=mesh, in_specs=placed, out_specs=rows, check_vma=False)
```

time: 134 us -> 113 us (0.84)
  Pallas kernels: 132 us -> 110 us
    pallas_call x1, Pallas kernels: 132 us -> 110 us  [on_device(): pl.pallas_call(kernel, out_shape=jax.ShapeDtypeStruct((n, D), bf16), in_s...]
where the time goes in v2:
time: 113 us; the launch traced here: 112 us
  Pallas kernels  110 us (97%)
  local copies, waits for them, and re-layouts  1.88 us (2%)
    pallas_call x1, Pallas kernels, on_device(): pl.pallas_call(kernel, out_shape=jax.ShapeDtypeStruct((n, D), bf16), in_s...  110 us

profile of v2, /device:TPU:0, one launch (start us, length us, event | category | flops | bytes accessed | tf_op | source)
XLA Modules:
  0.0 112.3 jit_solution(13451707869238383026)
XLA Ops:
  0.0 110.4 %shard_map.127 = bf16[128,2048]{1,0:T(8,128)(2,1)} custom-call(bf16[128,2048]{1,0:T(8,128)(2,1)} %tokens.1, bf16[128,2048]{1,0:T(8,128)(2,1)} %mixer.1, f32[1,2048]{1,0:T(1,128)} %bitcast.5, bf16[128,1280]{1,0:T(8,128)(2,1)} %w0.1, bf16[128,1280]{1,0:T(8,128)(2,1)} %w1.1, bf16[1280,128]{1,0:T(8,128)(2,1)} %w2.1, f32[1,2048]{1,0:T(1,128)} %bitcast.6, ...), custom_call_target="tpu_custom_call" | custom-call | tf_op jit(solution)/shard_map/pallas_call | solution.py:323
  110.4 1.9 %copy.15 = bf16[128,2048]{1,0:T(8,128)(2,1)} copy(bf16[128,2048]{1,0:T(8,128)(2,1)} %shard_map.127) | data formatting | bytes 1048576

commit v3 on v2

--- a/solution.py
+++ b/solution.py
@@ -14,42 +14,47 @@
 
 (
     OY1, OY2, OY3, OX1, OX2, F1, F2, X1, X3, QQ, E1, E2, OM, A2, A3, B2, C2, D1, D2, D3, D4, G1Z, G1ZM, G2Z,
-    G2ZM, G3Z, G3ZM, S2, SS, ADD, OWN, FIN, GATE0, VALUE0, DOWN0, GATE1, VALUE1, DOWN1,
-) = range(38)
+    G2ZM, G3Z, G3ZM, S2, SS, ADD, OWN, FIN, GATE0, VALUE0, DOWN0, GATE1, VALUE1, DOWN1, BASE, EARLY0,
+    EARLY1,
+) = range(41)
 
 ORDER = (
-    (G1Z, 0, 0), (G1ZM, 0, 0), (OY1, 0), (OM, 0), (OY2, 0), (OX1, 0), (OX2, 0), (G2Z, 0, 0), (G2ZM, 0, 0),
-    (OY3, 0), (OX1, 1), (OX2, 1), (G1Z, 0, 1), (G1ZM, 0, 1), (OY1, 1), (OM, 1), (OX1, 2), (A2, 0), (B2, 0),
-    (G3Z, 0, 0), (G3ZM, 0, 0), (OY2, 1), (X1, 0), (F1, 0), (OX2, 2), (A3, 0), (B2, 1), (G2Z, 0, 1),
-    (G2ZM, 0, 1), (F2, 0), (X3, 0), (G3Z, 0, 1), (G3ZM, 0, 1), (OY3, 1), (A2, 1), (D1, 0), (X1, 1), (B2, 2),
-    (F1, 1), (E1, 0), (C2, 0), (F2, 1), (E2, 0), (D3, 0), (QQ, 0), (OX1, 3), (A3, 1), (D1, 1), (QQ, 1), (X3, 1),
-    (OY1, 2), (OM, 2), (C2, 1), (D4, 0), (OY2, 2), (E1, 1), (D2, 0), (OY3, 2), (GATE0, 0, 1), (D2, 1), (E2, 1),
-    (GATE0, 1, 3), (OX2, 3), (GATE0, 3, 4), (D3, 1), (GATE0, 4, 5), (F1, 2), (OX1, 4), (A2, 2), (F2, 2),
-    (X1, 2), (D4, 1), (QQ, 2), (OX2, 4), (A3, 2), (VALUE0, 0, 1), (B2, 3), (VALUE0, 1, 2), (X3, 2), (OY1, 3),
-    (OM, 3), (VALUE0, 2, 4), (OY2, 3), (VALUE0, 4, 5), (C2, 2), (D1, 2), (DOWN0, 0), (S2, 0, 0, 0),
-    (SS, 0, 0, 0), (S2, 0, 0, 1), (SS, 0, 0, 1), (E1, 2), (OY3, 3), (DOWN0, 1), (D2, 2), (B2, 4), (S2, 0, 1, 0),
-    (SS, 0, 1, 0), (E2, 2), (SS, 0, 1, 1), (S2, 0, 1, 1), (ADD, 0, 0, 0), (F1, 3), (OX1, 5), (A2, 3), (D3, 2),
-    (ADD, 0, 0, 1), (F2, 3), (X1, 3), (ADD, 0, 1, 0), (DOWN0, 2), (S2, 0, 2, 0), (SS, 0, 2, 0), (SS, 0, 2, 1),
-    (QQ, 3), (OX2, 5), (A3, 3), (ADD, 0, 1, 1), (D4, 2), (S2, 0, 2, 1), (OY1, 4), (OM, 4), (OWN, 0, 0, 0),
-    (X3, 3), (OWN, 0, 1, 0), (DOWN0, 3), (S2, 0, 3, 0), (SS, 0, 3, 0), (SS, 0, 3, 1), (OY2, 4), (OWN, 0, 0, 1),
-    (C2, 3), (D1, 3), (S2, 0, 3, 1), (ADD, 0, 2, 0), (OY3, 4), (E1, 3), (D2, 3), (B2, 5), (ADD, 0, 2, 1),
-    (OWN, 0, 1, 1), (E2, 3), (ADD, 0, 3, 0), (F1, 4), (A2, 4), (X1, 4), (D3, 3), (ADD, 0, 3, 1), (OWN, 0, 2, 0),
-    (F2, 4), (OWN, 0, 3, 0), (FIN, 0, 0), (G1Z, 1, 0), (G1ZM, 1, 0), (QQ, 4), (OWN, 0, 2, 1), (A3, 4), (X3, 4),
-    (D4, 3), (OWN, 0, 3, 1), (FIN, 0, 1), (G2Z, 1, 0), (G2ZM, 1, 0), (OY1, 5), (OM, 5), (E1, 4), (D1, 4),
-    (OY2, 5), (G1Z, 1, 1), (G1ZM, 1, 1), (C2, 4), (E2, 4), (OY3, 5), (D2, 4), (D3, 4), (G3Z, 1, 0),
-    (G3ZM, 1, 0), (F1, 5), (A2, 5), (X1, 5), (G2Z, 1, 1), (G2ZM, 1, 1), (D4, 4), (F2, 5), (G3Z, 1, 1),
-    (G3ZM, 1, 1), (QQ, 5), (A3, 5), (X3, 5), (D1, 5), (GATE1, 0, 0, 4), (E1, 5), (GATE1, 0, 4, 5),
-    (VALUE1, 0, 0, 3), (C2, 5), (E2, 5), (VALUE1, 0, 3, 5), (DOWN1, 0, 0), (S2, 1, 0, 0), (SS, 1, 0, 0),
-    (DOWN1, 1, 0), (D2, 5), (D3, 5), (S2, 1, 1, 0), (SS, 1, 1, 0), (GATE1, 1, 0, 4), (DOWN1, 2, 0),
-    (S2, 1, 2, 0), (SS, 1, 2, 0), (GATE1, 1, 4, 5), (ADD, 1, 0, 0), (VALUE1, 1, 0, 1), (D4, 5),
-    (VALUE1, 1, 1, 3), (ADD, 1, 1, 0), (VALUE1, 1, 3, 5), (DOWN1, 3, 0), (ADD, 1, 2, 0), (S2, 1, 3, 0),
-    (SS, 1, 3, 0), (DOWN1, 0, 1), (SS, 1, 0, 1), (DOWN1, 1, 1), (S2, 1, 0, 1), (S2, 1, 1, 1), (DOWN1, 2, 1),
-    (OWN, 1, 0, 0), (DOWN1, 3, 1), (S2, 1, 2, 1), (S2, 1, 3, 1), (OWN, 1, 1, 0), (OWN, 1, 2, 0), (ADD, 1, 3, 0),
-    (SS, 1, 1, 1), (SS, 1, 3, 1), (SS, 1, 2, 1), (ADD, 1, 0, 1), (ADD, 1, 1, 1), (ADD, 1, 2, 1), (ADD, 1, 3, 1),
-    (OWN, 1, 3, 0), (FIN, 1, 0), (OWN, 1, 0, 1), (OWN, 1, 1, 1), (OWN, 1, 2, 1), (OWN, 1, 3, 1), (FIN, 1, 1),
+    (G1Z, 0, 0), (OY1, 0), (OM, 0), (G1ZM, 0, 1), (OX1, 0), (OY2, 0), (OX2, 0), (BASE,), (G1Z, 0, 1),
+    (G2ZM, 0, 1), (OY3, 0), (OX1, 1), (G2Z, 0, 1), (G1ZM, 0, 0), (OX2, 1), (A2, 0), (B2, 0), (F2, 0), (OX1, 2),
+    (G2Z, 0, 0), (G2ZM, 0, 0), (F1, 0), (X1, 0), (A3, 0), (B2, 1), (QQ, 0), (X3, 0), (G3Z, 0, 1), (G3ZM, 0, 1),
+    (OY1, 1), (OM, 1), (G3Z, 0, 0), (G3ZM, 0, 0), (C2, 0), (D1, 0), (OY2, 1), (E2, 0), (D2, 0), (OY3, 1),
+    (E1, 0), (D3, 0), (OX2, 2), (A2, 1), (F1, 1), (X1, 1), (D4, 0), (F2, 1), (OX1, 3), (A3, 1), (B2, 2),
+    (QQ, 1), (GATE0, 0, 1), (X3, 1), (GATE0, 1, 3), (D1, 1), (OY1, 2), (OM, 2), (GATE0, 3, 5), (C2, 1),
+    (OY2, 2), (E2, 1), (D2, 1), (EARLY0, 0, 1), (OY3, 2), (E1, 1), (EARLY0, 1, 4), (D3, 1), (OX2, 3),
+    (EARLY0, 4, 5), (A2, 2), (F2, 2), (X1, 2), (D4, 1), (F1, 2), (OX1, 4), (A3, 2), (B2, 3), (OY1, 3), (OM, 3),
+    (VALUE0, 0, 1), (X3, 2), (VALUE0, 1, 4), (D1, 2), (OY2, 3), (VALUE0, 4, 5), (DOWN0, 0), (SS, 0, 0, 1),
+    (SS, 0, 0, 0), (S2, 0, 0, 1), (S2, 0, 0, 0), (DOWN0, 1), (C2, 2), (SS, 0, 1, 1), (S2, 0, 1, 0), (E2, 2),
+    (QQ, 2), (S2, 0, 1, 1), (SS, 0, 1, 0), (F1, 3), (E1, 2), (ADD, 0, 0, 1), (A2, 3), (D3, 2), (OY3, 3),
+    (X1, 3), (ADD, 0, 0, 0), (D2, 2), (OX2, 4), (ADD, 0, 1, 0), (DOWN0, 2), (D4, 2), (ADD, 0, 1, 1),
+    (SS, 0, 2, 0), (S2, 0, 2, 0), (S2, 0, 2, 1), (E1, 3), (F2, 3), (SS, 0, 2, 1), (OWN, 0, 0, 1), (D1, 3),
+    (QQ, 3), (OX1, 5), (OWN, 0, 1, 0), (DOWN0, 3), (SS, 0, 3, 1), (S2, 0, 3, 0), (OWN, 0, 0, 0), (SS, 0, 3, 0),
+    (A3, 3), (B2, 4), (QQ, 4), (X3, 3), (OWN, 0, 1, 1), (S2, 0, 3, 1), (ADD, 0, 2, 0), (C2, 3), (OY1, 4),
+    (OM, 4), (ADD, 0, 2, 1), (D2, 3), (OY2, 4), (E2, 3), (ADD, 0, 3, 0), (D2, 4), (OY3, 4), (OX2, 5),
+    (ADD, 0, 3, 1), (OWN, 0, 2, 0), (D3, 3), (OWN, 0, 3, 0), (FIN, 0, 0), (G1ZM, 1, 0), (G1Z, 1, 0),
+    (OWN, 0, 2, 1), (A2, 4), (X1, 4), (D4, 3), (G2ZM, 1, 0), (G2Z, 1, 0), (F1, 4), (OWN, 0, 3, 1), (FIN, 0, 1),
+    (B2, 5), (F2, 4), (A3, 4), (X3, 4), (D1, 4), (OY1, 5), (OM, 5), (G3ZM, 1, 0), (G3Z, 1, 0), (OY2, 5),
+    (E1, 4), (G1ZM, 1, 1), (G1Z, 1, 1), (C2, 4), (OY3, 5), (E2, 4), (G2ZM, 1, 1), (G2Z, 1, 1), (D3, 4),
+    (GATE1, 0, 0, 3), (A2, 5), (F1, 5), (X1, 5), (GATE1, 0, 3, 5), (EARLY1, 0, 0, 3), (D4, 4), (G3Z, 1, 1),
+    (G3ZM, 1, 1), (F2, 5), (EARLY1, 0, 3, 5), (A3, 5), (X3, 5), (QQ, 5), (VALUE1, 0, 0, 1), (D1, 5),
+    (VALUE1, 0, 1, 5), (DOWN1, 0, 0), (SS, 1, 0, 0), (S2, 1, 0, 0), (E1, 5), (DOWN1, 1, 0), (SS, 1, 1, 0),
+    (S2, 1, 1, 0), (C2, 5), (E2, 5), (GATE1, 1, 0, 4), (D2, 5), (D3, 5), (ADD, 1, 0, 0), (GATE1, 1, 4, 5),
+    (EARLY1, 1, 0, 3), (ADD, 1, 1, 0), (EARLY1, 1, 3, 5), (VALUE1, 1, 0, 2), (DOWN1, 2, 0), (SS, 1, 2, 0),
+    (S2, 1, 2, 0), (VALUE1, 1, 2, 4), (D4, 5), (OWN, 1, 0, 0), (VALUE1, 1, 4, 5), (DOWN1, 0, 1), (S2, 1, 0, 1),
+    (SS, 1, 0, 1), (DOWN1, 1, 1), (SS, 1, 1, 1), (S2, 1, 1, 1), (DOWN1, 2, 1), (OWN, 1, 1, 0), (SS, 1, 2, 1),
+    (S2, 1, 2, 1), (DOWN1, 3, 0), (DOWN1, 3, 1), (ADD, 1, 2, 0), (S2, 1, 3, 0), (ADD, 1, 0, 1), (S2, 1, 3, 1),
+    (ADD, 1, 1, 1), (SS, 1, 3, 0), (ADD, 1, 2, 1), (ADD, 1, 3, 0), (OWN, 1, 2, 0), (SS, 1, 3, 1),
+    (ADD, 1, 3, 1), (OWN, 1, 0, 1), (OWN, 1, 1, 1), (OWN, 1, 3, 0), (FIN, 1, 0), (OWN, 1, 2, 1), (OWN, 1, 3, 1),
+    (FIN, 1, 1),
 )
 
 SETS = (((0, 0), (3, 0)), ((1, 0), (0, 1)), ((2, 0), (3, 1)), ((1, 1), (2, 1)))
+LATE = ((3, 1), (1, 1), (2, 1))
+EARLY = tuple(chip for chips in SETS for chip in chips if chip not in LATE)
 SET_OF = {chip: s for s, chips in enumerate(SETS) for chip in chips}
 STEPS = {
     OY1: ((), (("y+", (0, 0), 0, 1), ("y-", (0, 0), 2, 1)), "W1"),
@@ -86,7 +91,7 @@
 def kernel(
     tokens, mixer, early_norm, w0, w1, w2, early_post, mixer_gain, later_norm, w3, w4, w5, later_post,
     out,
-    g0, g1, g2, g3, g4, g5, rows0, rows1, gate_sum, hidden, part, base, branch, mixed, from_far, from_short, from_long,
+    g0, g1, g2, g3, g4, g5, rows0, rows1, gate_sum, value_sum, hidden, part, base, branch, mixed, from_far, from_short, from_long,
     w_send, w_recv, local_sem, z_send, z_recv,
 ):
     source = (w0, w1, w2, w3, w4, w5)
@@ -143,7 +148,6 @@
     for half in range(2):
         at = pl.ds(half * H, H)
         own_rows(0, half)[...] = rms_scale(tokens[at].astype(jnp.float32), early_norm[...]).astype(jnp.bfloat16)
-    base[...] = tokens[...].astype(jnp.float32) + rms_scale(mixer[...].astype(jnp.float32), mixer_gain[...])
     for m in range(MATRICES):
         local[m].wait()
     pl.semaphore_wait(barrier, len(where))
@@ -173,14 +177,11 @@
             need("w", (key, m), some(m, ARRIVALS[key]))
         for way, chip, first, quarters in moves:
             ref = piece(m, owner(chip, c), first, quarters)
-            key = arrival or ("mate", SET_OF[chip] if m % 3 == 2 else None)
+            key = arrival or ("mate", (None, chip in LATE, SET_OF[chip])[m % 3])
             send("w", ref, ref, m, (key, m), way)
 
-    def ready(m, s=None):
-        if s is None:
-            need("w", (("mate", None), m), some(m, 32))
-        else:
-            need("w", (("mate", s), m), some(m, 8))
+    def ready(m, s, shards):
+        need("w", (("mate", s), m), some(m, 4 * shards))
 
     def row_piece(layer, half, block, u):
         start = pl.multiple_of(half * M + block % T * H + u * U, U)
@@ -207,7 +208,7 @@
 
     def gate(layer, rows, first, last):
         weight = full[3 * layer]
-        ready(3 * layer)
+        ready(3 * layer, None, 8)
         for half in range(2) if rows is None else (rows,):
             all_gathered(layer, half)
 
@@ -218,20 +219,37 @@
                 all_rows[layer][span(rows)], weight[:, at], preferred_element_type=jnp.float32
             )
 
-    def value(layer, rows, first, last):
+    def partial_dot(layer, rows, weight, chips, at):
+        spots = [pl.ds(pl.multiple_of(owner(chip, 0) * 128, 256), 256) for chip in chips]
+        left = jnp.concatenate([all_rows[layer][span(rows), spot] for spot in spots], axis=1)
+        right = jnp.concatenate([weight[spot, at] for spot in spots], axis=0)
+        return jnp.dot(left, right, preferred_element_type=jnp.float32)
+
+    def value_early(layer, rows, first, last):
         weight = full[3 * layer + 1]
-        ready(3 * layer + 1)
+        ready(3 * layer + 1, False, len(EARLY))
+        for half in range(2) if rows is None else (rows,):
+            all_gathered(layer, half)
 
         @pl.loop(first, last)
         def _(j):
             at = pl.ds(pl.multiple_of(j * TILE, TILE), TILE)
-            b = jnp.dot(all_rows[layer][span(rows)], weight[:, at], preferred_element_type=jnp.float32)
+            value_sum[span(rows), at] = partial_dot(layer, rows, weight, EARLY, at)
+
+    def value(layer, rows, first, last):
+        weight = full[3 * layer + 1]
+        ready(3 * layer + 1, True, len(LATE))
+
+        @pl.loop(first, last)
+        def _(j):
+            at = pl.ds(pl.multiple_of(j * TILE, TILE), TILE)
+            b = value_sum[span(rows), at] + partial_dot(layer, rows, weight, LATE, at)
             a = gate_sum[span(rows), at]
             hidden[span(rows), at] = (a / (1.0 + jnp.exp(-a)) * b).astype(jnp.bfloat16)
 
     def down(layer, s, rows):
         weight = full[3 * layer + 2]
-        ready(3 * layer + 2, s)
+        ready(3 * layer + 2, s, 2)
         for k, chip in enumerate(SETS[s]):
             both = jnp.concatenate([weight[owner(chip, 0)], weight[owner(chip, 1)]], axis=1)
             sums = jnp.dot(hidden[span(rows)], both, preferred_element_type=jnp.float32)
@@ -272,6 +290,9 @@
             at = pl.ds(pl.multiple_of(owner(chip, 0) * (TILE // 2), TILE), TILE)
             branch[pl.ds(half * H, H), at] = total[:, k * TILE : (k + 1) * TILE]
 
+    def start_mixed():
+        base[...] = tokens[...].astype(jnp.float32) + rms_scale(mixer[...].astype(jnp.float32), mixer_gain[...])
+
     def finish(layer, half):
         at = pl.ds(half * H, H)
         if layer == 0:
@@ -285,9 +306,10 @@
 
     actions = {
         GATE0: lambda a, b: gate(0, None, a, b), VALUE0: lambda a, b: value(0, None, a, b),
+        EARLY0: lambda a, b: value_early(0, None, a, b), EARLY1: lambda h, a, b: value_early(1, h, a, b),
         GATE1: lambda h, a, b: gate(1, h, a, b), VALUE1: lambda h, a, b: value(1, h, a, b),
         DOWN0: lambda s: down(0, s, None), DOWN1: lambda s, h: down(1, s, h),
-        S2: sum_far, SS: sum_short, ADD: sum_long, OWN: sum_own, FIN: finish,
+        S2: sum_far, SS: sum_short, ADD: sum_long, OWN: sum_own, FIN: finish, BASE: start_mixed,
         G1Z: functools.partial(gather, 1, "z+"), G1ZM: functools.partial(gather, 1, "z-"),
         G2Z: functools.partial(gather, 2, "z+"), G2ZM: functools.partial(gather, 2, "z-"),
         G3Z: functools.partial(gather, 3, "z+"), G3ZM: functools.partial(gather, 3, "z-"),
@@ -318,7 +340,7 @@
     hbm = pl.BlockSpec(memory_space=pl.ANY)
     gathered = [pltpu.VMEM((F * depth, wide), bf16)] * 2 + [pltpu.VMEM((F,) + ed.shape, bf16)]
     landing = pltpu.VMEM((2, len(SETS), 2, H, 2 * TILE), bf16)
-    w_count = MATRICES * len(ARRIVALS) + 4 + 2 * len(SETS)
+    w_count = MATRICES * len(ARRIVALS) + 6 + 2 * len(SETS)
     z_count = 2 * 2 * (3 + 2 * len(SETS))
     return pl.pallas_call(
         kernel,
@@ -329,6 +351,7 @@
         + [
             pltpu.VMEM((T * n, D), bf16),
             pltpu.VMEM((T * n, D), bf16),
+            pltpu.VMEM((T * n, wide), f32),
             pltpu.VMEM((T * n, wide), f32),
             pltpu.VMEM((T * n, wide), bf16),
             pltpu.VMEM((2, len(SETS), T * n, 2 * TILE), bf16),

time: 113 us -> 110 us (0.973)
  Pallas kernels: 110 us -> 108 us
    pallas_call x1, Pallas kernels: 110 us -> 108 us  [on_device(): pl.pallas_call(kernel, out_shape=jax.ShapeDtypeStruct((n, D), bf16), in_s...]
where the time goes in v3:
time: 110 us
  Pallas kernels  108 us (98%)
  local copies, waits for them, and re-layouts  1.88 us (2%)
    pallas_call x1, Pallas kernels, on_device(): pl.pallas_call(kernel, out_shape=jax.ShapeDtypeStruct((n, D), bf16), in_s...  108 us

profile of v3, /device:TPU:0, one launch (start us, length us, event | category | flops | bytes accessed | tf_op | source)
XLA Modules:
  0.0 110.1 jit_solution(12006506624002458225)
XLA Ops:
  0.0 108.3 %shard_map.127 = bf16[128,2048]{1,0:T(8,128)(2,1)} custom-call(bf16[128,2048]{1,0:T(8,128)(2,1)} %tokens.1, bf16[128,2048]{1,0:T(8,128)(2,1)} %mixer.1, f32[1,2048]{1,0:T(1,128)} %bitcast.5, bf16[128,1280]{1,0:T(8,128)(2,1)} %w0.1, bf16[128,1280]{1,0:T(8,128)(2,1)} %w1.1, bf16[1280,128]{1,0:T(8,128)(2,1)} %w2.1, f32[1,2048]{1,0:T(1,128)} %bitcast.6, ...), custom_call_target="tpu_custom_call" | custom-call | tf_op jit(solution)/shard_map/pallas_call | solution.py:345
  108.3 1.9 %copy.15 = bf16[128,2048]{1,0:T(8,128)(2,1)} copy(bf16[128,2048]{1,0:T(8,128)(2,1)} %shard_map.127) | data formatting | bytes 1048576

commit v4 on v3

--- a/solution.py
+++ b/solution.py
@@ -89,8 +89,10 @@
 
 
 def kernel(
-    tokens, mixer, early_norm, w0, w1, w2, early_post, mixer_gain, later_norm, w3, w4, w5, later_post,
+    tokens_in, mixer_in, early_norm_in, w0, w1, w2, early_post_in, mixer_gain_in, later_norm_in, w3, w4, w5,
+    later_post_in,
     out,
+    tokens, mixer, early_norm, early_post, mixer_gain, later_norm, later_post,
     g0, g1, g2, g3, g4, g5, rows0, rows1, gate_sum, value_sum, hidden, part, base, branch, mixed, from_far, from_short, from_long,
     w_send, w_recv, local_sem, z_send, z_recv,
 ):
@@ -137,6 +139,13 @@
     barrier = pltpu.get_barrier_semaphore()
     for who in where.values():
         pl.semaphore_signal(barrier, inc=1, device_id=who, device_id_type=pl.DeviceIdType.MESH)
+    inputs = (
+        (tokens_in, tokens), (early_norm_in, early_norm), (mixer_in, mixer), (mixer_gain_in, mixer_gain),
+        (early_post_in, early_post), (later_norm_in, later_norm), (later_post_in, later_post),
+    )
+    loads = [pltpu.make_async_copy(*pair, local_sem.at[MATRICES + k]) for k, pair in enumerate(inputs)]
+    for load in loads:
+        load.start()
     local = []
     for m in range(MATRICES):
         local.append(pltpu.make_async_copy(source[m], piece(m, f, 0, 4), local_sem.at[m]))
@@ -145,11 +154,13 @@
     def own_rows(layer, half):
         return all_rows[layer].at[pl.ds(pl.multiple_of(half * M + t * H, H), H)]
 
+    for load in loads[:2]:
+        load.wait()
     for half in range(2):
         at = pl.ds(half * H, H)
         own_rows(0, half)[...] = rms_scale(tokens[at].astype(jnp.float32), early_norm[...]).astype(jnp.bfloat16)
-    for m in range(MATRICES):
-        local[m].wait()
+    for load in loads[2:] + local:
+        load.wait()
     pl.semaphore_wait(barrier, len(where))
 
     slots = {"w": {}, "z": {}}
@@ -344,10 +355,12 @@
     z_count = 2 * 2 * (3 + 2 * len(SETS))
     return pl.pallas_call(
         kernel,
-        out_shape=jax.ShapeDtypeStruct((n, D), bf16),
-        in_specs=[vmem] * 3 + [hbm] * 3 + [vmem] * 3 + [hbm] * 3 + [vmem],
+        out_shape=pltpu.VMEM((n, D), bf16),
+        in_specs=[hbm] * len(args),
         out_specs=vmem,
-        scratch_shapes=gathered * 2
+        scratch_shapes=[pltpu.VMEM((n, D), bf16)] * 2
+        + [pltpu.VMEM((1, D), f32)] * 5
+        + gathered * 2
         + [
             pltpu.VMEM((T * n, D), bf16),
             pltpu.VMEM((T * n, D), bf16),
@@ -363,7 +376,7 @@
             landing,
             pltpu.SemaphoreType.DMA((MATRICES,)),
             pltpu.SemaphoreType.DMA((w_count,)),
-            pltpu.SemaphoreType.DMA((MATRICES,)),
+            pltpu.SemaphoreType.DMA((MATRICES + 7,)),
             pltpu.SemaphoreType.DMA((4,)),
             pltpu.SemaphoreType.DMA((z_count,)),
         ],

time: 110 us -> 107 us (0.973)
    pallas_call x1, Pallas kernels: 108 us -> 107 us  [on_device(): pl.pallas_call(kernel, out_shape=pltpu.VMEM((n, D), bf16), in_specs=[hbm]...]
where the time goes in v4:
time: 107 us
  Pallas kernels  107 us (100%)
    pallas_call x1, Pallas kernels, on_device(): pl.pallas_call(kernel, out_shape=pltpu.VMEM((n, D), bf16), in_specs=[hbm]...  107 us

profile of v4, /device:TPU:0, one launch (start us, length us, event | category | flops | bytes accessed | tf_op | source)
XLA Modules:
  0.0 107.3 jit_solution(17267862456348937837)
XLA Ops:
  0.0 106.5 %shard_map.127 = bf16[128,2048]{1,0:T(8,128)(2,1)S(1)} custom-call(bf16[128,2048]{1,0:T(8,128)(2,1)} %tokens_in.1, bf16[128,2048]{1,0:T(8,128)(2,1)} %mixer_in.1, f32[1,2048]{1,0:T(1,128)} %bitcast.5, bf16[128,1280]{1,0:T(8,128)(2,1)} %w0.1, bf16[128,1280]{1,0:T(8,128)(2,1)} %w1.1, bf16[1280,128]{1,0:T(8,128)(2,1)} %w2.1, f32[1,2048]{1,0:T(1,128)} %bitcast.6, ...), custom_call_target="tpu_custom_call" | custom-call | tf_op jit(solution)/shard_map/pallas_call | solution.py:356
  106.5 0.8 copy.15

commit v5 on v4

--- a/solution.py
+++ b/solution.py
@@ -15,41 +15,41 @@
 (
     OY1, OY2, OY3, OX1, OX2, F1, F2, X1, X3, QQ, E1, E2, OM, A2, A3, B2, C2, D1, D2, D3, D4, G1Z, G1ZM, G2Z,
     G2ZM, G3Z, G3ZM, S2, SS, ADD, OWN, FIN, GATE0, VALUE0, DOWN0, GATE1, VALUE1, DOWN1, BASE, EARLY0,
-    EARLY1,
-) = range(41)
+    EARLY1, NORM,
+) = range(42)
 
 ORDER = (
-    (G1Z, 0, 0), (OY1, 0), (OM, 0), (G1ZM, 0, 1), (OX1, 0), (OY2, 0), (OX2, 0), (BASE,), (G1Z, 0, 1),
-    (G2ZM, 0, 1), (OY3, 0), (OX1, 1), (G2Z, 0, 1), (G1ZM, 0, 0), (OX2, 1), (A2, 0), (B2, 0), (F2, 0), (OX1, 2),
-    (G2Z, 0, 0), (G2ZM, 0, 0), (F1, 0), (X1, 0), (A3, 0), (B2, 1), (QQ, 0), (X3, 0), (G3Z, 0, 1), (G3ZM, 0, 1),
-    (OY1, 1), (OM, 1), (G3Z, 0, 0), (G3ZM, 0, 0), (C2, 0), (D1, 0), (OY2, 1), (E2, 0), (D2, 0), (OY3, 1),
-    (E1, 0), (D3, 0), (OX2, 2), (A2, 1), (F1, 1), (X1, 1), (D4, 0), (F2, 1), (OX1, 3), (A3, 1), (B2, 2),
-    (QQ, 1), (GATE0, 0, 1), (X3, 1), (GATE0, 1, 3), (D1, 1), (OY1, 2), (OM, 2), (GATE0, 3, 5), (C2, 1),
-    (OY2, 2), (E2, 1), (D2, 1), (EARLY0, 0, 1), (OY3, 2), (E1, 1), (EARLY0, 1, 4), (D3, 1), (OX2, 3),
-    (EARLY0, 4, 5), (A2, 2), (F2, 2), (X1, 2), (D4, 1), (F1, 2), (OX1, 4), (A3, 2), (B2, 3), (OY1, 3), (OM, 3),
-    (VALUE0, 0, 1), (X3, 2), (VALUE0, 1, 4), (D1, 2), (OY2, 3), (VALUE0, 4, 5), (DOWN0, 0), (SS, 0, 0, 1),
-    (SS, 0, 0, 0), (S2, 0, 0, 1), (S2, 0, 0, 0), (DOWN0, 1), (C2, 2), (SS, 0, 1, 1), (S2, 0, 1, 0), (E2, 2),
-    (QQ, 2), (S2, 0, 1, 1), (SS, 0, 1, 0), (F1, 3), (E1, 2), (ADD, 0, 0, 1), (A2, 3), (D3, 2), (OY3, 3),
-    (X1, 3), (ADD, 0, 0, 0), (D2, 2), (OX2, 4), (ADD, 0, 1, 0), (DOWN0, 2), (D4, 2), (ADD, 0, 1, 1),
-    (SS, 0, 2, 0), (S2, 0, 2, 0), (S2, 0, 2, 1), (E1, 3), (F2, 3), (SS, 0, 2, 1), (OWN, 0, 0, 1), (D1, 3),
-    (QQ, 3), (OX1, 5), (OWN, 0, 1, 0), (DOWN0, 3), (SS, 0, 3, 1), (S2, 0, 3, 0), (OWN, 0, 0, 0), (SS, 0, 3, 0),
-    (A3, 3), (B2, 4), (QQ, 4), (X3, 3), (OWN, 0, 1, 1), (S2, 0, 3, 1), (ADD, 0, 2, 0), (C2, 3), (OY1, 4),
-    (OM, 4), (ADD, 0, 2, 1), (D2, 3), (OY2, 4), (E2, 3), (ADD, 0, 3, 0), (D2, 4), (OY3, 4), (OX2, 5),
-    (ADD, 0, 3, 1), (OWN, 0, 2, 0), (D3, 3), (OWN, 0, 3, 0), (FIN, 0, 0), (G1ZM, 1, 0), (G1Z, 1, 0),
-    (OWN, 0, 2, 1), (A2, 4), (X1, 4), (D4, 3), (G2ZM, 1, 0), (G2Z, 1, 0), (F1, 4), (OWN, 0, 3, 1), (FIN, 0, 1),
-    (B2, 5), (F2, 4), (A3, 4), (X3, 4), (D1, 4), (OY1, 5), (OM, 5), (G3ZM, 1, 0), (G3Z, 1, 0), (OY2, 5),
-    (E1, 4), (G1ZM, 1, 1), (G1Z, 1, 1), (C2, 4), (OY3, 5), (E2, 4), (G2ZM, 1, 1), (G2Z, 1, 1), (D3, 4),
-    (GATE1, 0, 0, 3), (A2, 5), (F1, 5), (X1, 5), (GATE1, 0, 3, 5), (EARLY1, 0, 0, 3), (D4, 4), (G3Z, 1, 1),
-    (G3ZM, 1, 1), (F2, 5), (EARLY1, 0, 3, 5), (A3, 5), (X3, 5), (QQ, 5), (VALUE1, 0, 0, 1), (D1, 5),
-    (VALUE1, 0, 1, 5), (DOWN1, 0, 0), (SS, 1, 0, 0), (S2, 1, 0, 0), (E1, 5), (DOWN1, 1, 0), (SS, 1, 1, 0),
-    (S2, 1, 1, 0), (C2, 5), (E2, 5), (GATE1, 1, 0, 4), (D2, 5), (D3, 5), (ADD, 1, 0, 0), (GATE1, 1, 4, 5),
-    (EARLY1, 1, 0, 3), (ADD, 1, 1, 0), (EARLY1, 1, 3, 5), (VALUE1, 1, 0, 2), (DOWN1, 2, 0), (SS, 1, 2, 0),
-    (S2, 1, 2, 0), (VALUE1, 1, 2, 4), (D4, 5), (OWN, 1, 0, 0), (VALUE1, 1, 4, 5), (DOWN1, 0, 1), (S2, 1, 0, 1),
-    (SS, 1, 0, 1), (DOWN1, 1, 1), (SS, 1, 1, 1), (S2, 1, 1, 1), (DOWN1, 2, 1), (OWN, 1, 1, 0), (SS, 1, 2, 1),
-    (S2, 1, 2, 1), (DOWN1, 3, 0), (DOWN1, 3, 1), (ADD, 1, 2, 0), (S2, 1, 3, 0), (ADD, 1, 0, 1), (S2, 1, 3, 1),
-    (ADD, 1, 1, 1), (SS, 1, 3, 0), (ADD, 1, 2, 1), (ADD, 1, 3, 0), (OWN, 1, 2, 0), (SS, 1, 3, 1),
-    (ADD, 1, 3, 1), (OWN, 1, 0, 1), (OWN, 1, 1, 1), (OWN, 1, 3, 0), (FIN, 1, 0), (OWN, 1, 2, 1), (OWN, 1, 3, 1),
-    (FIN, 1, 1),
+    (OY1, 0), (OX1, 0), (OY2, 0), (OX2, 0), (NORM, 0), (G1Z, 0, 0), (G1ZM, 0, 0), (OY3, 0), (OM, 0), (NORM, 1),
+    (G1ZM, 0, 1), (G1Z, 0, 1), (G2ZM, 0, 1), (OX1, 1), (G2Z, 0, 1), (OX2, 1), (BASE,), (A2, 0), (B2, 0),
+    (F2, 0), (OX1, 2), (G2Z, 0, 0), (G2ZM, 0, 0), (F1, 0), (X1, 0), (A3, 0), (B2, 1), (QQ, 0), (X3, 0),
+    (G3Z, 0, 1), (G3ZM, 0, 1), (OY1, 1), (OM, 1), (G3Z, 0, 0), (G3ZM, 0, 0), (C2, 0), (D1, 0), (OY2, 1),
+    (E2, 0), (D2, 0), (OY3, 1), (E1, 0), (D3, 0), (OX2, 2), (A2, 1), (F1, 1), (X1, 1), (D4, 0), (F2, 1),
+    (OX1, 3), (A3, 1), (B2, 2), (QQ, 1), (GATE0, 0, 1), (X3, 1), (GATE0, 1, 3), (D1, 1), (OY1, 2), (OM, 2),
+    (GATE0, 3, 5), (C2, 1), (OY2, 2), (E2, 1), (D2, 1), (EARLY0, 0, 1), (OY3, 2), (E1, 1), (EARLY0, 1, 4),
+    (D3, 1), (OX2, 3), (EARLY0, 4, 5), (A2, 2), (F2, 2), (X1, 2), (D4, 1), (F1, 2), (OX1, 4), (A3, 2), (B2, 3),
+    (OY1, 3), (OM, 3), (VALUE0, 0, 1), (X3, 2), (VALUE0, 1, 4), (D1, 2), (OY2, 3), (VALUE0, 4, 5), (DOWN0, 0),
+    (SS, 0, 0, 1), (SS, 0, 0, 0), (S2, 0, 0, 1), (S2, 0, 0, 0), (DOWN0, 1), (C2, 2), (SS, 0, 1, 1),
+    (S2, 0, 1, 0), (E2, 2), (QQ, 2), (S2, 0, 1, 1), (SS, 0, 1, 0), (F1, 3), (E1, 2), (ADD, 0, 0, 1), (A2, 3),
+    (D3, 2), (OY3, 3), (X1, 3), (ADD, 0, 0, 0), (D2, 2), (OX2, 4), (ADD, 0, 1, 0), (DOWN0, 2), (D4, 2),
+    (ADD, 0, 1, 1), (SS, 0, 2, 0), (S2, 0, 2, 0), (S2, 0, 2, 1), (E1, 3), (F2, 3), (SS, 0, 2, 1),
+    (OWN, 0, 0, 1), (D1, 3), (QQ, 3), (OX1, 5), (OWN, 0, 1, 0), (DOWN0, 3), (SS, 0, 3, 1), (S2, 0, 3, 0),
+    (OWN, 0, 0, 0), (SS, 0, 3, 0), (A3, 3), (B2, 4), (QQ, 4), (X3, 3), (OWN, 0, 1, 1), (S2, 0, 3, 1),
+    (ADD, 0, 2, 0), (C2, 3), (OY1, 4), (OM, 4), (ADD, 0, 2, 1), (D2, 3), (OY2, 4), (E2, 3), (ADD, 0, 3, 0),
+    (D2, 4), (OY3, 4), (OX2, 5), (ADD, 0, 3, 1), (OWN, 0, 2, 0), (D3, 3), (OWN, 0, 3, 0), (FIN, 0, 0),
+    (G1ZM, 1, 0), (G1Z, 1, 0), (OWN, 0, 2, 1), (A2, 4), (X1, 4), (D4, 3), (G2ZM, 1, 0), (G2Z, 1, 0), (F1, 4),
+    (OWN, 0, 3, 1), (FIN, 0, 1), (B2, 5), (F2, 4), (A3, 4), (X3, 4), (D1, 4), (OY1, 5), (OM, 5), (G3ZM, 1, 0),
+    (G3Z, 1, 0), (OY2, 5), (E1, 4), (G1ZM, 1, 1), (G1Z, 1, 1), (C2, 4), (OY3, 5), (E2, 4), (G2ZM, 1, 1),
+    (G2Z, 1, 1), (D3, 4), (GATE1, 0, 0, 3), (A2, 5), (F1, 5), (X1, 5), (GATE1, 0, 3, 5), (EARLY1, 0, 0, 3),
+    (D4, 4), (G3Z, 1, 1), (G3ZM, 1, 1), (F2, 5), (EARLY1, 0, 3, 5), (A3, 5), (X3, 5), (QQ, 5),
+    (VALUE1, 0, 0, 1), (D1, 5), (VALUE1, 0, 1, 5), (DOWN1, 0, 0), (SS, 1, 0, 0), (S2, 1, 0, 0), (E1, 5),
+    (DOWN1, 1, 0), (SS, 1, 1, 0), (S2, 1, 1, 0), (C2, 5), (E2, 5), (GATE1, 1, 0, 4), (D2, 5), (D3, 5),
+    (ADD, 1, 0, 0), (GATE1, 1, 4, 5), (EARLY1, 1, 0, 3), (ADD, 1, 1, 0), (EARLY1, 1, 3, 5), (VALUE1, 1, 0, 2),
+    (DOWN1, 2, 0), (SS, 1, 2, 0), (S2, 1, 2, 0), (VALUE1, 1, 2, 4), (D4, 5), (OWN, 1, 0, 0), (VALUE1, 1, 4, 5),
+    (DOWN1, 0, 1), (S2, 1, 0, 1), (SS, 1, 0, 1), (DOWN1, 1, 1), (SS, 1, 1, 1), (S2, 1, 1, 1), (DOWN1, 2, 1),
+    (OWN, 1, 1, 0), (SS, 1, 2, 1), (S2, 1, 2, 1), (DOWN1, 3, 0), (DOWN1, 3, 1), (ADD, 1, 2, 0), (S2, 1, 3, 0),
+    (ADD, 1, 0, 1), (S2, 1, 3, 1), (ADD, 1, 1, 1), (SS, 1, 3, 0), (ADD, 1, 2, 1), (ADD, 1, 3, 0),
+    (OWN, 1, 2, 0), (SS, 1, 3, 1), (ADD, 1, 3, 1), (OWN, 1, 0, 1), (OWN, 1, 1, 1), (OWN, 1, 3, 0), (FIN, 1, 0),
+    (OWN, 1, 2, 1), (OWN, 1, 3, 1), (FIN, 1, 1),
 )
 
 SETS = (((0, 0), (3, 0)), ((1, 0), (0, 1)), ((2, 0), (3, 1)), ((1, 1), (2, 1)))
@@ -144,23 +144,22 @@
         (early_post_in, early_post), (later_norm_in, later_norm), (later_post_in, later_post),
     )
     loads = [pltpu.make_async_copy(*pair, local_sem.at[MATRICES + k]) for k, pair in enumerate(inputs)]
-    for load in loads:
+    local = [
+        pltpu.make_async_copy(source[m], piece(m, f, 0, 4), local_sem.at[m]) for m in range(MATRICES)
+    ]
+    for load in local[:1] + loads + local[1:]:
         load.start()
-    local = []
-    for m in range(MATRICES):
-        local.append(pltpu.make_async_copy(source[m], piece(m, f, 0, 4), local_sem.at[m]))
-        local[m].start()
+    loaded = set()
+
+    def load_wait(*copies):
+        for copy in copies:
+            if id(copy) not in loaded:
+                loaded.add(id(copy))
+                copy.wait()
 
     def own_rows(layer, half):
         return all_rows[layer].at[pl.ds(pl.multiple_of(half * M + t * H, H), H)]
 
-    for load in loads[:2]:
-        load.wait()
-    for half in range(2):
-        at = pl.ds(half * H, H)
-        own_rows(0, half)[...] = rms_scale(tokens[at].astype(jnp.float32), early_norm[...]).astype(jnp.bfloat16)
-    for load in loads[2:] + local:
-        load.wait()
     pl.semaphore_wait(barrier, len(where))
 
     slots = {"w": {}, "z": {}}
@@ -187,6 +186,8 @@
         for key in waits:
             need("w", (key, m), some(m, ARRIVALS[key]))
         for way, chip, first, quarters in moves:
+            if chip == (0, 0):
+                load_wait(local[m])
             ref = piece(m, owner(chip, c), first, quarters)
             key = arrival or ("mate", (None, chip in LATE, SET_OF[chip])[m % 3])
             send("w", ref, ref, m, (key, m), way)
@@ -301,7 +302,13 @@
             at = pl.ds(pl.multiple_of(owner(chip, 0) * (TILE // 2), TILE), TILE)
             branch[pl.ds(half * H, H), at] = total[:, k * TILE : (k + 1) * TILE]
 
+    def norm(half):
+        load_wait(*loads[:2])
+        at = pl.ds(half * H, H)
+        own_rows(0, half)[...] = rms_scale(tokens[at].astype(jnp.float32), early_norm[...]).astype(jnp.bfloat16)
+
     def start_mixed():
+        load_wait(*loads)
         base[...] = tokens[...].astype(jnp.float32) + rms_scale(mixer[...].astype(jnp.float32), mixer_gain[...])
 
     def finish(layer, half):
@@ -320,7 +327,7 @@
         EARLY0: lambda a, b: value_early(0, None, a, b), EARLY1: lambda h, a, b: value_early(1, h, a, b),
         GATE1: lambda h, a, b: gate(1, h, a, b), VALUE1: lambda h, a, b: value(1, h, a, b),
         DOWN0: lambda s: down(0, s, None), DOWN1: lambda s, h: down(1, s, h),
-        S2: sum_far, SS: sum_short, ADD: sum_long, OWN: sum_own, FIN: finish, BASE: start_mixed,
+        S2: sum_far, SS: sum_short, ADD: sum_long, OWN: sum_own, FIN: finish, BASE: start_mixed, NORM: norm,
         G1Z: functools.partial(gather, 1, "z+"), G1ZM: functools.partial(gather, 1, "z-"),
         G2Z: functools.partial(gather, 2, "z+"), G2ZM: functools.partial(gather, 2, "z-"),
         G3Z: functools.partial(gather, 3, "z+"), G3ZM: functools.partial(gather, 3, "z-"),

time: 107 us -> 107 us (level)
  no operation moved by 1% of the time
where the time goes in v5:
time: 107 us
  Pallas kernels  106 us (99%)
    pallas_call x1, Pallas kernels, on_device(): pl.pallas_call(kernel, out_shape=pltpu.VMEM((n, D), bf16), in_specs=[hbm]...  106 us

profile of v5, /device:TPU:0, one launch (start us, length us, event | category | flops | bytes accessed | tf_op | source)
XLA Modules:
  0.0 107.1 jit_solution(7078298990589157125)
XLA Ops:
  0.0 106.3 %shard_map.127 = bf16[128,2048]{1,0:T(8,128)(2,1)S(1)} custom-call(bf16[128,2048]{1,0:T(8,128)(2,1)} %tokens_in.1, bf16[128,2048]{1,0:T(8,128)(2,1)} %mixer_in.1, f32[1,2048]{1,0:T(1,128)} %bitcast.5, bf16[128,1280]{1,0:T(8,128)(2,1)} %w0.1, bf16[128,1280]{1,0:T(8,128)(2,1)} %w1.1, bf16[1280,128]{1,0:T(8,128)(2,1)} %w2.1, f32[1,2048]{1,0:T(1,128)} %bitcast.6, ...), custom_call_target="tpu_custom_call" | custom-call | tf_op jit(solution)/shard_map/pallas_call | solution.py:363
  106.3 0.8 copy.15

commit v6 on v5

--- a/solution.py
+++ b/solution.py
@@ -19,37 +19,37 @@
 ) = range(42)
 
 ORDER = (
-    (OY1, 0), (OX1, 0), (OY2, 0), (OX2, 0), (NORM, 0), (G1Z, 0, 0), (G1ZM, 0, 0), (OY3, 0), (OM, 0), (NORM, 1),
-    (G1ZM, 0, 1), (G1Z, 0, 1), (G2ZM, 0, 1), (OX1, 1), (G2Z, 0, 1), (OX2, 1), (BASE,), (A2, 0), (B2, 0),
-    (F2, 0), (OX1, 2), (G2Z, 0, 0), (G2ZM, 0, 0), (F1, 0), (X1, 0), (A3, 0), (B2, 1), (QQ, 0), (X3, 0),
-    (G3Z, 0, 1), (G3ZM, 0, 1), (OY1, 1), (OM, 1), (G3Z, 0, 0), (G3ZM, 0, 0), (C2, 0), (D1, 0), (OY2, 1),
-    (E2, 0), (D2, 0), (OY3, 1), (E1, 0), (D3, 0), (OX2, 2), (A2, 1), (F1, 1), (X1, 1), (D4, 0), (F2, 1),
-    (OX1, 3), (A3, 1), (B2, 2), (QQ, 1), (GATE0, 0, 1), (X3, 1), (GATE0, 1, 3), (D1, 1), (OY1, 2), (OM, 2),
-    (GATE0, 3, 5), (C2, 1), (OY2, 2), (E2, 1), (D2, 1), (EARLY0, 0, 1), (OY3, 2), (E1, 1), (EARLY0, 1, 4),
-    (D3, 1), (OX2, 3), (EARLY0, 4, 5), (A2, 2), (F2, 2), (X1, 2), (D4, 1), (F1, 2), (OX1, 4), (A3, 2), (B2, 3),
-    (OY1, 3), (OM, 3), (VALUE0, 0, 1), (X3, 2), (VALUE0, 1, 4), (D1, 2), (OY2, 3), (VALUE0, 4, 5), (DOWN0, 0),
-    (SS, 0, 0, 1), (SS, 0, 0, 0), (S2, 0, 0, 1), (S2, 0, 0, 0), (DOWN0, 1), (C2, 2), (SS, 0, 1, 1),
-    (S2, 0, 1, 0), (E2, 2), (QQ, 2), (S2, 0, 1, 1), (SS, 0, 1, 0), (F1, 3), (E1, 2), (ADD, 0, 0, 1), (A2, 3),
-    (D3, 2), (OY3, 3), (X1, 3), (ADD, 0, 0, 0), (D2, 2), (OX2, 4), (ADD, 0, 1, 0), (DOWN0, 2), (D4, 2),
-    (ADD, 0, 1, 1), (SS, 0, 2, 0), (S2, 0, 2, 0), (S2, 0, 2, 1), (E1, 3), (F2, 3), (SS, 0, 2, 1),
-    (OWN, 0, 0, 1), (D1, 3), (QQ, 3), (OX1, 5), (OWN, 0, 1, 0), (DOWN0, 3), (SS, 0, 3, 1), (S2, 0, 3, 0),
-    (OWN, 0, 0, 0), (SS, 0, 3, 0), (A3, 3), (B2, 4), (QQ, 4), (X3, 3), (OWN, 0, 1, 1), (S2, 0, 3, 1),
-    (ADD, 0, 2, 0), (C2, 3), (OY1, 4), (OM, 4), (ADD, 0, 2, 1), (D2, 3), (OY2, 4), (E2, 3), (ADD, 0, 3, 0),
-    (D2, 4), (OY3, 4), (OX2, 5), (ADD, 0, 3, 1), (OWN, 0, 2, 0), (D3, 3), (OWN, 0, 3, 0), (FIN, 0, 0),
-    (G1ZM, 1, 0), (G1Z, 1, 0), (OWN, 0, 2, 1), (A2, 4), (X1, 4), (D4, 3), (G2ZM, 1, 0), (G2Z, 1, 0), (F1, 4),
-    (OWN, 0, 3, 1), (FIN, 0, 1), (B2, 5), (F2, 4), (A3, 4), (X3, 4), (D1, 4), (OY1, 5), (OM, 5), (G3ZM, 1, 0),
-    (G3Z, 1, 0), (OY2, 5), (E1, 4), (G1ZM, 1, 1), (G1Z, 1, 1), (C2, 4), (OY3, 5), (E2, 4), (G2ZM, 1, 1),
-    (G2Z, 1, 1), (D3, 4), (GATE1, 0, 0, 3), (A2, 5), (F1, 5), (X1, 5), (GATE1, 0, 3, 5), (EARLY1, 0, 0, 3),
-    (D4, 4), (G3Z, 1, 1), (G3ZM, 1, 1), (F2, 5), (EARLY1, 0, 3, 5), (A3, 5), (X3, 5), (QQ, 5),
+    (OY1, 0), (OM, 0), (OX1, 0), (OY2, 0), (OX2, 0), (NORM, 0), (G1Z, 0, 0), (G1ZM, 0, 0), (NORM, 1),
+    (G1Z, 0, 1), (G1ZM, 0, 1), (BASE,), (OY3, 0), (OX1, 1), (G2Z, 0, 1), (G2ZM, 0, 1), (OX2, 1), (A2, 0),
+    (F2, 0), (B2, 0), (OX1, 2), (G2Z, 0, 0), (G2ZM, 0, 0), (F1, 0), (X1, 0), (G3Z, 0, 1), (G3ZM, 0, 1), (A3, 0),
+    (QQ, 0), (B2, 1), (X3, 0), (OY1, 1), (OM, 1), (G3Z, 0, 0), (G3ZM, 0, 0), (C2, 0), (OY2, 1), (D1, 0),
+    (E2, 0), (D2, 0), (OY3, 1), (E1, 0), (D3, 0), (OX2, 2), (A2, 1), (F1, 1), (X1, 1), (QQ, 1), (D4, 0),
+    (OX1, 3), (GATE0, 0, 1), (A3, 1), (B2, 2), (F2, 1), (X3, 1), (GATE0, 1, 3), (D1, 1), (OY1, 2), (OM, 2),
+    (GATE0, 3, 5), (D2, 1), (OY2, 2), (E1, 1), (C2, 1), (OY3, 2), (E2, 1), (EARLY0, 0, 1), (D3, 1), (OX2, 3),
+    (EARLY0, 1, 4), (A2, 2), (X1, 2), (F2, 2), (EARLY0, 4, 5), (F1, 2), (D4, 1), (OX1, 4), (VALUE0, 0, 1),
+    (A3, 2), (B2, 3), (X3, 2), (OY1, 3), (OM, 3), (VALUE0, 1, 4), (D1, 2), (OY2, 3), (VALUE0, 4, 5), (DOWN0, 0),
+    (SS, 0, 0, 1), (SS, 0, 0, 0), (S2, 0, 0, 1), (S2, 0, 0, 0), (DOWN0, 1), (C2, 2), (E2, 2), (S2, 0, 1, 0),
+    (SS, 0, 1, 1), (QQ, 2), (S2, 0, 1, 1), (SS, 0, 1, 0), (F1, 3), (E1, 2), (ADD, 0, 0, 1), (A2, 3), (OY3, 3),
+    (D3, 2), (X1, 3), (ADD, 0, 0, 0), (D2, 2), (OX2, 4), (ADD, 0, 1, 0), (DOWN0, 2), (D4, 2), (ADD, 0, 1, 1),
+    (SS, 0, 2, 0), (S2, 0, 2, 0), (S2, 0, 2, 1), (SS, 0, 2, 1), (F2, 3), (E1, 3), (OWN, 0, 0, 1), (QQ, 3),
+    (D1, 3), (OX1, 5), (OWN, 0, 1, 0), (DOWN0, 3), (S2, 0, 3, 0), (SS, 0, 3, 1), (SS, 0, 3, 0), (OWN, 0, 0, 0),
+    (S2, 0, 3, 1), (A3, 3), (OY1, 4), (OM, 4), (B2, 4), (X3, 3), (OWN, 0, 1, 1), (ADD, 0, 2, 0), (C2, 3),
+    (QQ, 4), (ADD, 0, 2, 1), (D2, 3), (OY2, 4), (E2, 3), (ADD, 0, 3, 0), (OY3, 4), (OX2, 5), (ADD, 0, 3, 1),
+    (OWN, 0, 2, 0), (D2, 4), (D3, 3), (OWN, 0, 2, 1), (OWN, 0, 3, 0), (FIN, 0, 0), (G1Z, 1, 0), (G1ZM, 1, 0),
+    (G2ZM, 1, 0), (G2Z, 1, 0), (A2, 4), (X1, 4), (D4, 3), (F1, 4), (OWN, 0, 3, 1), (FIN, 0, 1), (F2, 4),
+    (B2, 5), (A3, 4), (X3, 4), (OY1, 5), (OM, 5), (D1, 4), (G3Z, 1, 0), (G3ZM, 1, 0), (G1Z, 1, 1), (G1ZM, 1, 1),
+    (OY2, 5), (E1, 4), (C2, 4), (OY3, 5), (E2, 4), (G2Z, 1, 1), (G2ZM, 1, 1), (D3, 4), (GATE1, 0, 0, 2),
+    (A2, 5), (X1, 5), (F1, 5), (GATE1, 0, 2, 5), (EARLY1, 0, 0, 1), (F2, 5), (EARLY1, 0, 1, 2), (D4, 4),
+    (EARLY1, 0, 2, 3), (G3ZM, 1, 1), (G3Z, 1, 1), (EARLY1, 0, 3, 5), (A3, 5), (X3, 5), (QQ, 5),
     (VALUE1, 0, 0, 1), (D1, 5), (VALUE1, 0, 1, 5), (DOWN1, 0, 0), (SS, 1, 0, 0), (S2, 1, 0, 0), (E1, 5),
-    (DOWN1, 1, 0), (SS, 1, 1, 0), (S2, 1, 1, 0), (C2, 5), (E2, 5), (GATE1, 1, 0, 4), (D2, 5), (D3, 5),
-    (ADD, 1, 0, 0), (GATE1, 1, 4, 5), (EARLY1, 1, 0, 3), (ADD, 1, 1, 0), (EARLY1, 1, 3, 5), (VALUE1, 1, 0, 2),
-    (DOWN1, 2, 0), (SS, 1, 2, 0), (S2, 1, 2, 0), (VALUE1, 1, 2, 4), (D4, 5), (OWN, 1, 0, 0), (VALUE1, 1, 4, 5),
-    (DOWN1, 0, 1), (S2, 1, 0, 1), (SS, 1, 0, 1), (DOWN1, 1, 1), (SS, 1, 1, 1), (S2, 1, 1, 1), (DOWN1, 2, 1),
-    (OWN, 1, 1, 0), (SS, 1, 2, 1), (S2, 1, 2, 1), (DOWN1, 3, 0), (DOWN1, 3, 1), (ADD, 1, 2, 0), (S2, 1, 3, 0),
-    (ADD, 1, 0, 1), (S2, 1, 3, 1), (ADD, 1, 1, 1), (SS, 1, 3, 0), (ADD, 1, 2, 1), (ADD, 1, 3, 0),
-    (OWN, 1, 2, 0), (SS, 1, 3, 1), (ADD, 1, 3, 1), (OWN, 1, 0, 1), (OWN, 1, 1, 1), (OWN, 1, 3, 0), (FIN, 1, 0),
-    (OWN, 1, 2, 1), (OWN, 1, 3, 1), (FIN, 1, 1),
+    (DOWN1, 1, 0), (SS, 1, 1, 0), (S2, 1, 1, 0), (C2, 5), (E2, 5), (GATE1, 1, 0, 3), (D2, 5), (D3, 5),
+    (GATE1, 1, 3, 4), (ADD, 1, 0, 0), (GATE1, 1, 4, 5), (EARLY1, 1, 0, 3), (ADD, 1, 1, 0), (EARLY1, 1, 3, 4),
+    (DOWN1, 2, 0), (SS, 1, 2, 0), (S2, 1, 2, 0), (EARLY1, 1, 4, 5), (VALUE1, 1, 0, 3), (D4, 5),
+    (VALUE1, 1, 3, 4), (OWN, 1, 0, 0), (VALUE1, 1, 4, 5), (DOWN1, 0, 1), (SS, 1, 0, 1), (S2, 1, 0, 1),
+    (DOWN1, 1, 1), (S2, 1, 1, 1), (SS, 1, 1, 1), (DOWN1, 2, 1), (SS, 1, 2, 1), (S2, 1, 2, 1), (OWN, 1, 1, 0),
+    (DOWN1, 3, 0), (DOWN1, 3, 1), (ADD, 1, 2, 0), (S2, 1, 3, 0), (SS, 1, 3, 0), (S2, 1, 3, 1), (ADD, 1, 0, 1),
+    (ADD, 1, 1, 1), (SS, 1, 3, 1), (ADD, 1, 2, 1), (OWN, 1, 2, 0), (ADD, 1, 3, 0), (ADD, 1, 3, 1),
+    (OWN, 1, 0, 1), (OWN, 1, 1, 1), (OWN, 1, 3, 0), (FIN, 1, 0), (OWN, 1, 2, 1), (OWN, 1, 3, 1), (FIN, 1, 1),
 )
 
 SETS = (((0, 0), (3, 0)), ((1, 0), (0, 1)), ((2, 0), (3, 1)), ((1, 1), (2, 1)))

time: 107 us -> 107 us (level)
  no operation moved by 1% of the time
where the time goes in v6:
time: 107 us
  Pallas kernels  106 us (99%)
    pallas_call x1, Pallas kernels, on_device(): pl.pallas_call(kernel, out_shape=pltpu.VMEM((n, D), bf16), in_specs=[hbm]...  106 us

profile of v6, /device:TPU:0, one launch (start us, length us, event | category | flops | bytes accessed | tf_op | source)
XLA Modules:
  0.0 106.6 jit_solution(612185186038527844)
XLA Ops:
  0.0 105.8 %shard_map.127 = bf16[128,2048]{1,0:T(8,128)(2,1)S(1)} custom-call(bf16[128,2048]{1,0:T(8,128)(2,1)} %tokens_in.1, bf16[128,2048]{1,0:T(8,128)(2,1)} %mixer_in.1, f32[1,2048]{1,0:T(1,128)} %bitcast.5, bf16[128,1280]{1,0:T(8,128)(2,1)} %w0.1, bf16[128,1280]{1,0:T(8,128)(2,1)} %w1.1, bf16[1280,128]{1,0:T(8,128)(2,1)} %w2.1, f32[1,2048]{1,0:T(1,128)} %bitcast.6, ...), custom_call_target="tpu_custom_call" | custom-call | tf_op jit(solution)/shard_map/pallas_call | solution.py:363
  105.8 0.8 copy.15

commit v7 on v6

--- a/solution.py
+++ b/solution.py
@@ -31,23 +31,22 @@
     (SS, 0, 0, 1), (SS, 0, 0, 0), (S2, 0, 0, 1), (S2, 0, 0, 0), (DOWN0, 1), (C2, 2), (E2, 2), (S2, 0, 1, 0),
     (SS, 0, 1, 1), (QQ, 2), (S2, 0, 1, 1), (SS, 0, 1, 0), (F1, 3), (E1, 2), (ADD, 0, 0, 1), (A2, 3), (OY3, 3),
     (D3, 2), (X1, 3), (ADD, 0, 0, 0), (D2, 2), (OX2, 4), (ADD, 0, 1, 0), (DOWN0, 2), (D4, 2), (ADD, 0, 1, 1),
-    (SS, 0, 2, 0), (S2, 0, 2, 0), (S2, 0, 2, 1), (SS, 0, 2, 1), (F2, 3), (E1, 3), (OWN, 0, 0, 1), (QQ, 3),
-    (D1, 3), (OX1, 5), (OWN, 0, 1, 0), (DOWN0, 3), (S2, 0, 3, 0), (SS, 0, 3, 1), (SS, 0, 3, 0), (OWN, 0, 0, 0),
-    (S2, 0, 3, 1), (A3, 3), (OY1, 4), (OM, 4), (B2, 4), (X3, 3), (OWN, 0, 1, 1), (ADD, 0, 2, 0), (C2, 3),
+    (SS, 0, 2, 0), (S2, 0, 2, 0), (S2, 0, 2, 1), (SS, 0, 2, 1), (F2, 3), (E1, 3), (OWN, 0, 0, 1), (D1, 3),
+    (QQ, 3), (OX1, 5), (DOWN0, 3), (S2, 0, 3, 0), (SS, 0, 3, 1), (SS, 0, 3, 0), (OWN, 0, 1, 0), (S2, 0, 3, 1),
+    (OWN, 0, 0, 0), (A3, 3), (OY1, 4), (OM, 4), (B2, 4), (X3, 3), (OWN, 0, 1, 1), (ADD, 0, 2, 0), (C2, 3),
     (QQ, 4), (ADD, 0, 2, 1), (D2, 3), (OY2, 4), (E2, 3), (ADD, 0, 3, 0), (OY3, 4), (OX2, 5), (ADD, 0, 3, 1),
     (OWN, 0, 2, 0), (D2, 4), (D3, 3), (OWN, 0, 2, 1), (OWN, 0, 3, 0), (FIN, 0, 0), (G1Z, 1, 0), (G1ZM, 1, 0),
     (G2ZM, 1, 0), (G2Z, 1, 0), (A2, 4), (X1, 4), (D4, 3), (F1, 4), (OWN, 0, 3, 1), (FIN, 0, 1), (F2, 4),
-    (B2, 5), (A3, 4), (X3, 4), (OY1, 5), (OM, 5), (D1, 4), (G3Z, 1, 0), (G3ZM, 1, 0), (G1Z, 1, 1), (G1ZM, 1, 1),
-    (OY2, 5), (E1, 4), (C2, 4), (OY3, 5), (E2, 4), (G2Z, 1, 1), (G2ZM, 1, 1), (D3, 4), (GATE1, 0, 0, 2),
-    (A2, 5), (X1, 5), (F1, 5), (GATE1, 0, 2, 5), (EARLY1, 0, 0, 1), (F2, 5), (EARLY1, 0, 1, 2), (D4, 4),
-    (EARLY1, 0, 2, 3), (G3ZM, 1, 1), (G3Z, 1, 1), (EARLY1, 0, 3, 5), (A3, 5), (X3, 5), (QQ, 5),
-    (VALUE1, 0, 0, 1), (D1, 5), (VALUE1, 0, 1, 5), (DOWN1, 0, 0), (SS, 1, 0, 0), (S2, 1, 0, 0), (E1, 5),
-    (DOWN1, 1, 0), (SS, 1, 1, 0), (S2, 1, 1, 0), (C2, 5), (E2, 5), (GATE1, 1, 0, 3), (D2, 5), (D3, 5),
-    (GATE1, 1, 3, 4), (ADD, 1, 0, 0), (GATE1, 1, 4, 5), (EARLY1, 1, 0, 3), (ADD, 1, 1, 0), (EARLY1, 1, 3, 4),
-    (DOWN1, 2, 0), (SS, 1, 2, 0), (S2, 1, 2, 0), (EARLY1, 1, 4, 5), (VALUE1, 1, 0, 3), (D4, 5),
-    (VALUE1, 1, 3, 4), (OWN, 1, 0, 0), (VALUE1, 1, 4, 5), (DOWN1, 0, 1), (SS, 1, 0, 1), (S2, 1, 0, 1),
+    (B2, 5), (A3, 4), (X3, 4), (OY1, 5), (OM, 5), (D1, 4), (G3Z, 1, 0), (G3ZM, 1, 0), (OY2, 5), (G1Z, 1, 1),
+    (G1ZM, 1, 1), (E1, 4), (C2, 4), (OY3, 5), (E2, 4), (G2Z, 1, 1), (G2ZM, 1, 1), (D3, 4), (GATE1, 0, 0, 1),
+    (A2, 5), (X1, 5), (F1, 5), (GATE1, 0, 1, 5), (F2, 5), (EARLY1, 0, 0, 1), (D4, 4), (EARLY1, 0, 1, 3),
+    (G3ZM, 1, 1), (G3Z, 1, 1), (EARLY1, 0, 3, 5), (A3, 5), (X3, 5), (QQ, 5), (D1, 5), (VALUE1, 0, 0, 5),
+    (DOWN1, 0, 0), (SS, 1, 0, 0), (S2, 1, 0, 0), (E1, 5), (DOWN1, 1, 0), (SS, 1, 1, 0), (S2, 1, 1, 0), (C2, 5),
+    (E2, 5), (GATE1, 1, 0, 2), (D2, 5), (D3, 5), (GATE1, 1, 2, 4), (ADD, 1, 0, 0), (GATE1, 1, 4, 5),
+    (EARLY1, 1, 0, 3), (ADD, 1, 1, 0), (DOWN1, 2, 0), (SS, 1, 2, 0), (S2, 1, 2, 0), (EARLY1, 1, 3, 5),
+    (VALUE1, 1, 0, 2), (D4, 5), (VALUE1, 1, 2, 5), (OWN, 1, 0, 0), (DOWN1, 0, 1), (SS, 1, 0, 1), (S2, 1, 0, 1),
     (DOWN1, 1, 1), (S2, 1, 1, 1), (SS, 1, 1, 1), (DOWN1, 2, 1), (SS, 1, 2, 1), (S2, 1, 2, 1), (OWN, 1, 1, 0),
-    (DOWN1, 3, 0), (DOWN1, 3, 1), (ADD, 1, 2, 0), (S2, 1, 3, 0), (SS, 1, 3, 0), (S2, 1, 3, 1), (ADD, 1, 0, 1),
+    (DOWN1, 3, 0), (ADD, 1, 2, 0), (DOWN1, 3, 1), (S2, 1, 3, 0), (SS, 1, 3, 0), (S2, 1, 3, 1), (ADD, 1, 0, 1),
     (ADD, 1, 1, 1), (SS, 1, 3, 1), (ADD, 1, 2, 1), (OWN, 1, 2, 0), (ADD, 1, 3, 0), (ADD, 1, 3, 1),
     (OWN, 1, 0, 1), (OWN, 1, 1, 1), (OWN, 1, 3, 0), (FIN, 1, 0), (OWN, 1, 2, 1), (OWN, 1, 3, 1), (FIN, 1, 1),
 )

time: 107 us -> 107 us (level)
  no operation moved by 1% of the time
where the time goes in v7:
time: 107 us
  Pallas kernels  106 us (99%)
    pallas_call x1, Pallas kernels, on_device(): pl.pallas_call(kernel, out_shape=pltpu.VMEM((n, D), bf16), in_specs=[hbm]...  106 us

profile of v7, /device:TPU:0, one launch (start us, length us, event | category | flops | bytes accessed | tf_op | source)
XLA Modules:
  0.0 106.6 jit_solution(8238654660822420339)
XLA Ops:
  0.0 105.8 %shard_map.127 = bf16[128,2048]{1,0:T(8,128)(2,1)S(1)} custom-call(bf16[128,2048]{1,0:T(8,128)(2,1)} %tokens_in.1, bf16[128,2048]{1,0:T(8,128)(2,1)} %mixer_in.1, f32[1,2048]{1,0:T(1,128)} %bitcast.5, bf16[128,1280]{1,0:T(8,128)(2,1)} %w0.1, bf16[128,1280]{1,0:T(8,128)(2,1)} %w1.1, bf16[1280,128]{1,0:T(8,128)(2,1)} %w2.1, f32[1,2048]{1,0:T(1,128)} %bitcast.6, ...), custom_call_target="tpu_custom_call" | custom-call | tf_op jit(solution)/shard_map/pallas_call | solution.py:362
  105.8 0.8 copy.15
